TPU v7x, 32 devices: a whole 2x2x4 slice. The times are simulated.
32 devices in a mesh: sp: 8 (over z, y), tp: 4 (over x, core).
Axes of the slice: x: 2, y: 2, z: 4, core: 2. Of those that a mesh axis runs over, the one named last changes fastest.
Arguments:
- tokens: bfloat16 [2048, 4096], P(('sp', 'tp')), may hold values from -6 to 6
- norm_gain: float32 [4096], replicated, may hold values from 0.1 to 1.9
- w_query: bfloat16 [4096, 1024], P(None, 'tp'), may hold values from -0.25 to 0.25
- w_key: bfloat16 [4096, 512], P(None, 'tp'), may hold values from -0.09375 to 0.09375
- w_value: bfloat16 [4096, 512], P(None, 'tp'), may hold values from -0.09375 to 0.09375
- score_shift: float32 [8], P('tp'), may hold values from -15 to -8
- w_conv_b: bfloat16 [4096, 1024], P(None, 'tp'), may hold values from -0.09375 to 0.09375
- w_conv_c: bfloat16 [4096, 1024], P(None, 'tp'), may hold values from -0.09375 to 0.09375
- w_conv_u: bfloat16 [4096, 1024], P(None, 'tp'), may hold values from -0.09375 to 0.09375
- conv_kernel: float32 [3, 1024], P(None, 'tp'), may hold values from -3.5 to 3.5
- w_out_att: bfloat16 [4096, 1024], P('sp', 'tp'), may hold values from -0.75 to 0.75
- w_out_conv: bfloat16 [4096, 1024], P('sp', 'tp'), may hold values from -0.1875 to 0.1875
Outputs:
- mixed: bfloat16 [2048, 4096], P(('sp', 'tp'))
- log_weight: float32 [2048, 8], P('sp', 'tp')
All inputs are finite; a program needn't handle non-finite values.
Results may differ from a plain program's by a relative error of at most 0.017.
Values may be sent and summed in bfloat16 or wider, within the bound.
A program may use at most 128 MiB of HBM per device.

v0:
```python
import functools

import jax
import jax.numpy as jnp
from jax import lax
from jax.experimental import pallas as pl
from jax.experimental.pallas import tpu as pltpu
from jax.sharding import PartitionSpec as P

HEAD_DIM = 128
CONV_K = 3
HALO = 16
F32 = jnp.float32
BF16 = jnp.bfloat16
MESH = pl.DeviceIdType.MESH
NT = (((1,), (1,)), ((), ()))


def softplus(z):
    u = jnp.exp(-jnp.abs(z))
    small = u * (1.0 - u * (0.5 - u * (1.0 / 3.0 - u * 0.25)))
    return jnp.maximum(z, 0.0) + jnp.where(u < 0.01, small, jnp.log(1.0 + u))


def kernel(
    n,
    tok_ref, gain_ref, wq_hbm, wk_hbm, wv_hbm, shift_ref, wb_hbm, wc_hbm, wu_hbm, taps_ref, woa_ref, woc_ref,
    out_ref, logw_ref,
    wq, wk, wv, wb, wc, wu, xall, normed, q_sc, kv, wo, gate_sc, prod_sc, prev, ext, attn, conv, partial, totals,
    snd, keep, d2d, xsnd, xrcv,
    load_sem, tok_ssem, tok_rsem, kv_sem, w_sem, halo_sem, d2d_sem, x_sem,
):
    sp = lax.axis_index("sp")
    t = lax.axis_index("tp")
    near = t + 1 - 2 * (t % 2)
    far = t + 2 - 4 * ((t // 2) % 2)
    diag = near + 2 - 4 * ((near // 2) % 2)
    pos = jnp.where(sp % 2 == 0, sp // 2, n - 1 - sp // 2)

    def ring(place):
        place = (place + 2 * n) % n
        return jnp.where(place < n // 2, 2 * place, 2 * (n - 1 - place) + 1)

    right, left = ring(pos + 1), ring(pos - 1)
    following, leading = (sp + 1) % n, (sp + n - 1) % n
    rows = tok_ref.shape[0]
    toks = 4 * rows
    half = rows // 2
    fpart = wo.shape[2] // 2
    heads = q_sc.shape[1] // HEAD_DIM
    kv_cols = kv.shape[4]
    grouping = heads // (kv_cols // HEAD_DIM)

    loads = [
        pltpu.make_async_copy(src, dst, load_sem.at[i])
        for i, (src, dst) in enumerate(
            ((wk_hbm, wk), (wv_hbm, wv), (wq_hbm, wq), (wc_hbm, wc), (wu_hbm, wu), (wb_hbm, wb))
        )
    ]
    own_loads = [
        pltpu.make_async_copy(src, wo.at[sp, i], load_sem.at[6 + i]) for i, src in enumerate((woa_ref, woc_ref))
    ]
    barrier = pltpu.get_barrier_semaphore()
    for place in (right, left, following, leading):
        pl.semaphore_signal(barrier, inc=1, device_id={"sp": place}, device_id_type=MESH)
    for place in (near, far):
        pl.semaphore_signal(barrier, inc=1, device_id={"tp": place}, device_id_type=MESH)
    for load in (*own_loads, *loads):
        load.start()
    pl.semaphore_wait(barrier, 6)

    def push(src, dst, ssem, rsem, who):
        return pltpu.make_async_remote_copy(
            src_ref=src, dst_ref=dst, send_sem=ssem, recv_sem=rsem, device_id=who, device_id_type=MESH
        )

    to_far = [
        push(tok_ref.at[pl.ds(c * half, half)], xall.at[t, pl.ds(c * half, half)], tok_ssem.at[c], tok_rsem.at[c], {"tp": far})
        for c in range(2)
    ]
    to_near = push(tok_ref, xall.at[t], tok_ssem.at[2], tok_rsem.at[2], {"tp": near})
    relay = [
        push(xall.at[far, pl.ds(c * half, half)], xall.at[far, pl.ds(c * half, half)], tok_ssem.at[3 + c], tok_rsem.at[3 + c], {"tp": near})
        for c in range(2)
    ]
    for copy in to_far:
        copy.start()
    to_near.start()

    last = n // 2

    def hop(part, sem, way, step, chunk):
        block = ring(pos - (step - 1)) if way == 0 else ring(pos + (step - 1))
        view = part(block, chunk, step)
        return push(
            view[0], view[1], sem.at[0, way, step - 1, chunk], sem.at[1, way, step - 1, chunk],
            {"sp": right if way == 0 else left},
        )

    def ways(step, chunk, chunks):
        if isinstance(step, int) and step == last:
            return (0,) if chunk < chunks // 2 else (1,)
        return (0, 1)

    early = t // 2

    def kv_part(block, chunk, step):
        view = kv.at[block, early + chunk * (1 - 2 * early)]
        return view, view

    def w_part(block, chunk, step):
        view = wo.at[block, chunk // 2, pl.ds(pl.multiple_of((chunk % 2) * fpart, fpart), fpart)]
        return view, view

    rings = {"kv": (kv_part, kv_sem, 2), "w": (w_part, w_sem, 4)}

    def emit(name, step, chunk):
        part, sem, chunks = rings[name]
        for way in ways(step, chunk, chunks):
            hop(part, sem, way, step, chunk).start()

    def take(name, step, chunk, onward=None):
        part, sem, chunks = rings[name]
        for way in ways(step, chunk, chunks):
            hop(part, sem, way, step, chunk).wait_recv()
        if onward or (onward is None and step < last):
            emit(name, step + 1, chunk)

    for load in own_loads:
        load.wait()
    for chunk in (0, 1):
        emit("w", 1, chunk)

    def dot(w):
        return jnp.dot(normed[...], w[...], preferred_element_type=F32).astype(BF16)

    def project_kv(groups, pair):
        for i, g in enumerate(groups):
            x = (tok_ref[...] if g is None else xall[g]).astype(F32)
            inverse = lax.rsqrt(jnp.mean(x * x, axis=-1, keepdims=True) + 1e-06)
            at = rows * (t % 2 if i == 0 else 1 - t % 2)
            normed[pl.ds(pl.multiple_of(at, rows), rows)] = (x * inverse * gain_ref[...]).astype(BF16)
        kv[sp, pair, 0] = dot(wk)
        kv[sp, pair, 1] = dot(wv)

    def project_rest(pair):
        at = pl.ds(pl.multiple_of(pair * 2 * rows, 2 * rows), 2 * rows)
        prod_sc[at] = (dot(wc).astype(F32) * dot(wu).astype(F32)).astype(BF16)
        q_sc[at] = dot(wq)
        gate_sc[at] = dot(wb)

    to_near.wait_recv()
    for load in loads[:2]:
        load.wait()
    project_kv((None, near), early)
    emit("kv", 1, 0)
    for chunk in (2, 3):
        emit("w", 1, chunk)
    for load in loads[2:]:
        load.wait()
    project_rest(early)
    to_far[0].wait_recv()
    relay[0].start()
    take("kv", 1, 0)
    take("w", 1, 0)
    to_far[1].wait_recv()
    relay[1].start()
    for c in range(2):
        relay[c].wait_recv()
    project_kv((far, diag), 1 - early)
    emit("kv", 1, 1)
    take("w", 1, 1)
    take("w", 1, 2)
    project_rest(1 - early)
    halo = push(prod_sc.at[pl.ds(toks - HALO, HALO)], prev, halo_sem.at[0], halo_sem.at[1], {"sp": following})
    halo.start()

    key_i = lax.broadcasted_iota(jnp.int32, (toks, toks), 0)
    key_j = lax.broadcasted_iota(jnp.int32, (toks, toks), 1)
    later = (key_i > key_j).astype(F32).astype(BF16)
    lane = lax.broadcasted_iota(jnp.int32, (toks, totals.shape[2]), 1)
    scale = HEAD_DIM ** (-0.5)
    order = (t, far, near, diag)

    def visit(slot, masked):
        for h in range(heads):
            cols = pl.ds(h * HEAD_DIM, HEAD_DIM)
            kv_at = pl.ds((h // grouping) * HEAD_DIM, HEAD_DIM)
            keys = kv[slot, :, 0, :, kv_at].reshape(toks, HEAD_DIM)
            vals = kv[slot, :, 1, :, kv_at].reshape(toks, HEAD_DIM)
            z = lax.dot_general(q_sc[:, cols], keys, NT, preferred_element_type=F32) * scale + shift_ref[0, h]
            soft = softplus(z)
            if masked:
                soft = jnp.where(key_j < key_i, soft, 0.0)
            high = soft.astype(BF16)
            low = (soft - high.astype(F32)).astype(BF16)
            after = jnp.dot(high, later, preferred_element_type=F32) + jnp.dot(low, later, preferred_element_type=F32)
            weight = jnp.exp(z - soft - after)
            if masked:
                weight = jnp.where(key_j < key_i, weight, 0.0)
            partial[slot, :, cols] = jnp.dot(weight.astype(BF16), vals, preferred_element_type=F32)
            total = after[:, 0:1] + soft[:, 0:1]
            totals[h] = jnp.where(lane == slot, total, totals[h])

    def visit_at(step, both=True):
        def side(i, carry):
            slot = ring(pos + (2 * i - 1) * step)

            @pl.when(slot < sp)
            def _():
                visit(slot, False)

            return carry

        lax.fori_loop(0, 2 if both else 1, side, 0)

    totals[...] = jnp.zeros(totals.shape, F32)
    visit(sp, True)

    def w_event(m):
        return m // 4 + 1, m % 4

    def body(s, carry):
        if n > 4:
            take("kv", s + 1, 0, True)
            take("kv", s, 1, True)
            take("w", *w_event(2 * s + 1), True)
            take("w", *w_event(2 * s + 2), True)
            visit_at(s)
        return carry

    def convolve():
        halo.wait_recv()
        ext[pl.ds(HALO, toks)] = prod_sc[...].astype(F32)
        ext[pl.ds(0, HALO)] = jnp.where(sp == 0, 0.0, prev[...].astype(F32))
        summed = jnp.zeros((toks, ext.shape[1]), F32)
        for tap in range(CONV_K):
            summed = summed + taps_ref[tap : tap + 1, :] * ext[pl.ds(HALO - (CONV_K - 1) + tap, toks)]
        ext[pl.ds(HALO, toks)] = gate_sc[...].astype(F32) * summed
        for i, g in enumerate(order):
            conv[pl.ds(i * rows, rows)] = ext[pl.ds(pl.multiple_of(HALO + g * rows, HALO), rows)].astype(BF16)

    loops = max(last - 3, 0)
    lax.fori_loop(1, 1 + loops, body, 0)
    w_done = 3 + 2 * loops
    convolve()
    for s in range(1 + loops, last + 1):
        if s + 1 <= last:
            take("kv", s + 1, 0)
        take("kv", s, 1)
        for m in range(w_done, w_done + 2 if s < last else w_done + 1):
            take("w", *w_event(m))
            w_done += 1
        visit_at(s, s < last)

    def combine(i, carry):
        slot = sp - i
        suffixes = []
        for h in range(heads):
            cols = pl.ds(h * HEAD_DIM, HEAD_DIM)
            suffix = carry[h]
            ext[pl.ds(HALO, toks), cols] += jnp.exp(-suffix) * partial[slot, :, cols]
            total = jnp.sum(jnp.where(lane == slot, totals[h], 0.0), axis=1, keepdims=True)
            suffixes.append(suffix + total)
        return tuple(suffixes)

    ext[...] = jnp.zeros(ext.shape, F32)
    suffixes = lax.fori_loop(0, sp + 1, combine, tuple(jnp.zeros((toks, 1), F32) for _ in range(heads)))
    for h in range(heads):
        spread = jnp.broadcast_to(suffixes[h], (toks, 128)).T[0:1, :]
        logw_ref[h : h + 1, :] = jnp.log(jnp.maximum(1.0 - jnp.exp(-spread), 0.05))
    for i, g in enumerate(order):
        attn[pl.ds(i * rows, rows)] = ext[pl.ds(pl.multiple_of(HALO + g * rows, HALO), rows), 0 : attn.shape[1]].astype(BF16)

    def block_of(i):
        return ring(pos - (i + 1) // 2) if i % 2 else ring(pos + i // 2)

    def d2d_copy(i):
        return push(snd.at[i], d2d.at[i], d2d_sem.at[0, i], d2d_sem.at[1, i], {"tp": near})

    def x_copy(i):
        return push(xsnd.at[i], xrcv.at[i], x_sem.at[0, i], x_sem.at[1, i], {"tp": far})

    def first(i):
        j = block_of(i)
        share = lax.dot_general(attn[...], wo[j, 0], NT, preferred_element_type=F32)
        share = (share + lax.dot_general(conv[...], wo[j, 1], NT, preferred_element_type=F32)).astype(BF16)
        snd[i] = share[2 * rows :]
        keep[i] = share[: 2 * rows]
        d2d_copy(i).start()

    def second(i):
        d2d_copy(i).wait_recv()
        xsnd[i] = (keep[i, pl.ds(rows, rows)].astype(F32) + d2d[i, pl.ds(rows, rows)].astype(F32)).astype(BF16)
        x_copy(i).start()

    def third(i):
        x_copy(i).wait_recv()
        own = keep[i, pl.ds(0, rows)].astype(F32) + d2d[i, pl.ds(0, rows)].astype(F32)
        done = (own + xrcv[i].astype(F32)).astype(BF16)
        if len(out_ref.shape) == 3:
            out_ref[block_of(i)] = done
        else:
            feats = keep.shape[2]
            out_ref[:, pl.ds(pl.multiple_of(block_of(i) * feats, feats), feats)] = done

    for i in range(n):
        while w_done < max(4 * ((i + 1) // 2), min(10 + i, 4 * last)):
            take("w", *w_event(w_done))
            w_done += 1
        first(i)
        if i >= 1:
            second(i - 1)
        if i >= 3:
            third(i - 3)
    second(n - 1)
    for i in range(max(n - 3, 0), n):
        third(i)

    for copy in (*to_far, to_near, *relay, halo):
        copy.wait_send()
    for part, sem, chunks in rings.values():
        for step in range(1, last + 1):
            for chunk in range(chunks):
                for way in ways(step, chunk, chunks):
                    hop(part, sem, way, step, chunk).wait_send()
    for i in range(n):
        d2d_copy(i).wait_send()
        x_copy(i).wait_send()


def local(
    n, tokens, norm_gain, w_query, w_key, w_value, score_shift, w_conv_b, w_conv_c, w_conv_u,
    conv_kernel, w_out_att, w_out_conv,
):
    rows, d = tokens.shape
    toks = 4 * rows
    feats, att_cols = w_out_att.shape
    conv_cols = w_out_conv.shape[1]
    heads = score_shift.shape[0]
    kv_cols = w_key.shape[1]
    vmem = pl.BlockSpec(memory_space=pltpu.VMEM)
    smem = pl.BlockSpec(memory_space=pltpu.SMEM)
    hbm = pl.BlockSpec(memory_space=pl.ANY)
    dma = pltpu.SemaphoreType.DMA
    wide = feats % 128 == 0
    out, logw = pl.pallas_call(
        functools.partial(kernel, n),
        out_shape=(
            jax.ShapeDtypeStruct((rows, n * feats) if wide else (n, rows, feats), BF16),
            jax.ShapeDtypeStruct((heads, toks), F32),
        ),
        in_specs=[vmem, vmem, hbm, hbm, hbm, smem, hbm, hbm, hbm, vmem, hbm, hbm],
        out_specs=(vmem, vmem),
        scratch_shapes=[
            *[pltpu.VMEM(w.shape, BF16) for w in (w_query, w_key, w_value, w_conv_b, w_conv_c, w_conv_u)],
            pltpu.VMEM((4, rows, d), BF16),
            pltpu.VMEM((2 * rows, d), BF16),
            pltpu.VMEM((toks, w_query.shape[1]), BF16),
            pltpu.VMEM((n, 2, 2, 2 * rows, kv_cols), BF16),
            pltpu.VMEM((n, 2, feats, att_cols), BF16),
            pltpu.VMEM((toks, conv_cols), BF16),
            pltpu.VMEM((toks, conv_cols), BF16),
            pltpu.VMEM((HALO, conv_cols), BF16),
            pltpu.VMEM((toks + HALO, max(conv_cols, att_cols)), F32),
            pltpu.VMEM((toks, att_cols), BF16),
            pltpu.VMEM((toks, conv_cols), BF16),
            pltpu.VMEM((n, toks, att_cols), F32),
            pltpu.VMEM((heads, toks, 128), F32),
            pltpu.VMEM((n, 2 * rows, feats), BF16),
            pltpu.VMEM((n, 2 * rows, feats), BF16),
            pltpu.VMEM((n, 2 * rows, feats), BF16),
            pltpu.VMEM((n, rows, feats), BF16),
            pltpu.VMEM((n, rows, feats), BF16),
            dma((8,)), dma((5,)), dma((5,)), dma((2, 2, n // 2, 2)), dma((2, 2, n // 2, 4)), dma((2,)), dma((2, n)), dma((2, n)),
        ],
        compiler_params=pltpu.CompilerParams(
            collective_id=0, has_side_effects=True, vmem_limit_bytes=60 * 1024 * 1024
        ),
    )(
        tokens, norm_gain.reshape(1, d), w_query, w_key, w_value, score_shift.reshape(1, heads),
        w_conv_b, w_conv_c, w_conv_u, conv_kernel, w_out_att, w_out_conv,
    )
    if not wide:
        out = out.transpose(1, 0, 2).reshape(rows, n * feats)
    return (out, logw.T)


def solution(mesh):
    return jax.shard_map(
        functools.partial(local, mesh.shape["sp"]),
        mesh=mesh,
        in_specs=(
            P(("sp", "tp"), None), P(), P(None, "tp"), P(None, "tp"), P(None, "tp"), P("tp"),
            P(None, "tp"), P(None, "tp"), P(None, "tp"), P(None, "tp"), P("sp", "tp"), P("sp", "tp"),
        ),
        out_specs=(P(("sp", "tp"), None), P("sp", "tp")),
        check_vma=False,
    )
```

profile of v0, /device:TPU:9, one launch (start us, length us, event | category | flops | bytes accessed | tf_op | source)
XLA Modules:
  0.0 71.6 jit_solution(13906588492352835162)
XLA Ops:
  0.6 67.9 %shard_map.131 = (bf16[64,4096]{1,0:T(8,128)(2,1)}, f32[2,256]{1,0:T(2,128)}) custom-call(bf16[64,4096]{1,0:T(8,128)(2,1)} %tok_ref.1, f32[1,4096]{1,0:T(1,128)} %bitcast.3, bf16[4096,256]{1,0:T(8,128)(2,1)} %wq_hbm.1, bf16[4096,128]{1,0:T(8,128)(2,1)} %wk_hbm.1, bf16[4096,128]{1,0:T(8,128)(2,1)} %wv_hbm.1, f32[1,2]{1,0:T(1,128)} %bitcast.5, ...), custom_call_target="tpu_custom_call" | custom-call | tf_op jit(solution)/shard_map/pallas_call | solution.py:347
  68.5 1.9 %copy.16 = bf16[64,4096]{1,0:T(8,128)(2,1)} copy(bf16[64,4096]{1,0:T(8,128)(2,1)} %get-tuple-element.8) | data formatting | bytes 1048576
  70.4 1.3 %copy.17 = f32[256,2]{0,1:T(2,128)} copy(f32[256,2]{0,1:T(2,128)} %bitcast.4) | data formatting | bytes 4096
where the time goes:
time: 71.8 us; the launch traced here: 71.6 us
  Pallas kernels  67.9 us (95%)
  local copies, waits for them, and re-layouts  3.12 us (4%)
    pallas_call x1, Pallas kernels, local(): pl.pallas_call(functools.partial(kernel, n), out_shape=(jax.ShapeDtypeStr...  67.9 us
    unnamed x2, local copies, waits for them, and re-layouts  3.12 us

commit v1 on v0

--- a/solution.py
+++ b/solution.py
@@ -14,6 +14,69 @@
 BF16 = jnp.bfloat16
 MESH = pl.DeviceIdType.MESH
 NT = (((1,), (1,)), ((), ()))
+W_OWN = [(5, 1, 6, 7, 7, 3, 6, 2), (5, 5, 4, 7, 3, 3, 6, 6), (5, 5, 7, 7, 7, 5, 6, 6), (5, 5, 7, 6, 3, 7, 6, 6)]
+W_EVENTS = [[],
+ [],
+ [(73, 1, 1, 68, 386, 193, 260, 324), (132, 192, 195, 129, -1, 258, 458, 386), (-1, -1, 256, 326, -1, 454, -1, -1)],
+ [],
+ [],
+ [(81, 9, 8, 73, 394, 205, 268, 332),
+  (148, 204, 200, 139, 338, 458, -1, 394),
+  (89, 212, 270, 334, -1, -1, -1, -1),
+  (156, -1, 278, 350, -1, -1, -1, -1)],
+ [(192, 17, 208, 144, 402, 272, 466, 340),
+  (200, 216, 286, 258, 149, 466, 276, -1),
+  (-1, 24, 16, 80, 344, -1, 474, -1),
+  (-1, -1, 219, -1, -1, -1, -1, -1)],
+ [],
+ [(208, 324, 384, 152, 410, 209, -1, 402), (268, -1, -1, 452, 157, 474, -1, -1), (-1, -1, -1, -1, 449, -1, -1, -1)],
+ [(-1, 128, 28, 88, -1, -1, 284, 348), (-1, -1, 67, -1, -1, -1, -1, -1)],
+ [(-1, -1, -1, -1, -1, -1, 322, -1)],
+ [(276, 140, 392, 264, 456, 145, -1, 410), (-1, -1, -1, 460, 4, 133, -1, -1), (-1, -1, -1, -1, 200, 386, -1, -1)],
+ [(-1, 144, 72, 0, -1, -1, 144, 192), (-1, -1, 320, -1, -1, -1, 330, -1)],
+ [(-1, 332, 338, 272, 466, 76, -1, 256), (-1, -1, -1, 464, -1, 394, -1, -1)],
+ [(-1, -1, -1, -1, 193, -1, -1, -1)],
+ [(-1, -1, -1, 9, -1, -1, -1, 204)],
+ [(-1, -1, -1, -1, 129, 141, -1, 266)],
+ [(-1, -1, -1, -1, -1, 152, -1, -1)],
+ [],
+ [],
+ [(320, -1, 81, -1, -1, -1, 156, -1), (-1, -1, 328, -1, -1, -1, 336, -1)],
+ [(280, -1, -1, 282, -1, -1, -1, -1), (136, -1, -1, 472, -1, -1, -1, -1)],
+ [(216, 152, -1, -1, 474, 402, 448, -1)],
+ [(328, -1, 400, 17, 72, 0, 344, 212),
+  (64, -1, -1, -1, 320, 408, -1, 144),
+  (-1, -1, -1, -1, 136, -1, -1, 272),
+  (-1, -1, -1, -1, 221, -1, -1, 128),
+  (-1, -1, -1, -1, -1, -1, -1, 282)],
+ [(344, 348, 89, -1, 328, 264, 192, 140),
+  (340, 260, 344, -1, -1, 12, 200, 152),
+  (-1, 264, -1, -1, -1, 216, 128, -1),
+  (-1, 272, -1, -1, -1, -1, 210, -1),
+  (-1, 280, -1, -1, -1, -1, 220, -1)],
+ [(256, 337, -1, 384, 68, 20, 136, 216),
+  (-1, -1, -1, 25, 84, 64, -1, -1),
+  (-1, -1, -1, 392, 8, 28, -1, -1),
+  (-1, -1, -1, -1, 92, -1, -1, -1)],
+ [(-1, -1, 412, 400, 16, 280, -1, -1), (-1, -1, -1, 408, 208, -1, -1, -1)],
+ [(-1, -1, 448, 336, 24, 80, -1, -1),
+  (-1, -1, 464, -1, -1, 88, -1, -1),
+  (-1, -1, 456, -1, -1, -1, -1, -1),
+  (-1, -1, 472, -1, -1, -1, -1, -1)],
+ [],
+ []]
+CELLS = [(0, 1, 2, 3, 4, 5, 6, 7),
+ (2, 3, 4, 2, 6, 7, 4, 5),
+ (3, 0, 3, 1, 7, 2, 7, 6),
+ (1, 2, 0, 4, 2, 6, 5, 4),
+ (5, 4, 1, 7, 5, 3, 3, 2),
+ (4, 5, 5, 0, 1, 0, 2, 3),
+ (-1, -1, 6, 6, 3, 4, -1, -1),
+ (-1, -1, 7, 5, 0, 1, -1, -1),
+ (-1, -1, 6, 6, 0, 0, -1, -1),
+ (-1, -1, 7, 7, 1, 1, -1, -1)]
+CELL_BACK = [(6, 6, -1, -1, -1, -1, 0, 0), (7, 7, -1, -1, -1, -1, 1, 1)]
+CELL_ORDER = (0, 1, 2, 3, 4, 5, 6, 7, 8, 9)
 
 
 def softplus(z):
@@ -385,10 +448,450 @@
         out = out.transpose(1, 0, 2).reshape(rows, n * feats)
     return (out, logw.T)
 
+def grid_kernel(
+    n,
+    tok_ref, gain_ref, wq_hbm, wk_hbm, wv_hbm, shift_ref, wb_hbm, wc_hbm, wu_hbm, taps_ref, woa_ref, woc_ref,
+    out_ref, logw_ref,
+    wq, wkv, wb, wc, wu, xall, normed, q_sc, kv, wo, gate_sc, prod_sc, prev, ext, attn, conv, acc, suffix,
+    snd, keep, d2d, xsnd, xrcv, guest, gsnd, grcv,
+    load_sem, tok_ssem, tok_rsem, kv_ssem, kv_fsem, kv_rsem, w_ssem, w_rsem, halo_sem, d2d_sem, x_sem,
+    act_sem, ret_sem, near_by, further,
+):
+    sp = lax.axis_index("sp")
+    t = lax.axis_index("tp")
+    z = sp // 2
+    y = sp % 2
+    near = t + 1 - 2 * (t % 2)
+    far = t + 2 - 4 * ((t // 2) % 2)
+    diag = near + 2 - 4 * ((near // 2) % 2)
+    up, down, side = sp + 2, sp - 2, sp + 1 - 2 * y
+    ways = (up, down, side)
+    host = sp + 2 - 4 * (z % 2)
+    levels = n // 2
+    has_up, has_down = z < levels - 1, z > 0
+    outer = jnp.logical_or(z == 0, z == levels - 1)
+    inner = jnp.logical_and(z > 0, z < levels - 1)
+    rows = tok_ref.shape[0]
+    toks = 4 * rows
+    half = rows // 2
+    fpart = wo.shape[2] // 2
+    feats = wo.shape[2]
+    heads = q_sc.shape[1] // HEAD_DIM
+    kv_cols = kv.shape[4]
+    grouping = heads // (kv_cols // HEAD_DIM)
+
+    def pick(vals):
+        out = vals[0]
+        for i in range(1, n):
+            if vals[i] != vals[0] or not isinstance(out, int):
+                out = jnp.where(sp == i, vals[i], out)
+        return out
+
+    def guard(cond):
+        return pl.when(cond)
+
+    loads = [
+        pltpu.make_async_copy(src, dst, load_sem.at[i])
+        for i, (src, dst) in enumerate(
+            (
+                (wk_hbm, wkv.at[:, pl.ds(0, kv_cols)]), (wv_hbm, wkv.at[:, pl.ds(kv_cols, kv_cols)]),
+                (wc_hbm, wc), (wu_hbm, wu), (wq_hbm, wq), (wb_hbm, wb),
+            )
+        )
+    ]
+    own_loads = [
+        pltpu.make_async_copy(src, wo.at[sp, i], load_sem.at[6 + i]) for i, src in enumerate((woa_ref, woc_ref))
+    ]
+    barrier = pltpu.get_barrier_semaphore()
+
+    def tell(sem, place):
+        pl.semaphore_signal(sem, inc=1, device_id={"sp": place}, device_id_type=MESH)
+
+    def tell_column(sem):
+        guard(has_up)(lambda: tell(sem, up))
+        guard(has_down)(lambda: tell(sem, down))
+
+    column = has_up.astype(jnp.int32) + has_down.astype(jnp.int32)
+    for place in (near, far):
+        pl.semaphore_signal(barrier, inc=1, device_id={"tp": place}, device_id_type=MESH)
+    tell(barrier, side)
+    tell_column(barrier)
+    for load in (*own_loads, *loads):
+        load.start()
+    pl.semaphore_wait(barrier, 3 + column)
+
+    def push(src, dst, ssem, rsem, who):
+        return pltpu.make_async_remote_copy(
+            src_ref=src, dst_ref=dst, send_sem=ssem, recv_sem=rsem, device_id=who, device_id_type=MESH
+        )
+
+    to_far = [
+        push(tok_ref.at[pl.ds(c * half, half)], xall.at[t, pl.ds(c * half, half)], tok_ssem.at[c], tok_rsem.at[c], {"tp": far})
+        for c in range(2)
+    ]
+    to_near = push(tok_ref, xall.at[t], tok_ssem.at[2], tok_rsem.at[2], {"tp": near})
+    relay = [
+        push(xall.at[far, pl.ds(c * half, half)], xall.at[far, pl.ds(c * half, half)], tok_ssem.at[3 + c], tok_rsem.at[3 + c], {"tp": near})
+        for c in range(2)
+    ]
+    for copy in to_far:
+        copy.start()
+    to_near.start()
+    tell_column(near_by)
+
+    def w_copy(h, c, d):
+        view = wo.at[h, c // 2, pl.ds(pl.multiple_of((c % 2) * fpart, fpart), fpart)]
+        return push(view, view, w_ssem.at[d, h, c], w_rsem.at[h, c], {"sp": ways[d]})
+
+    def w_spread(vals, act):
+        code = pick(vals)
+        for d in range(3):
+            if any(v >= 0 and v // 2**d % 2 for v in vals):
+                guard(jnp.logical_and(code >= 0, code // 2**d % 2 == 1))(
+                    lambda d=d: act(w_copy(code // 64, code // 8 % 8, d))
+                )
+
+    def w_own(c, act):
+        mask = pick(W_OWN[c])
+        for d in range(3):
+            if any(v // 2**d % 2 for v in W_OWN[c]):
+                guard(mask // 2**d % 2 == 1)(lambda d=d: act(w_copy(sp, c, d)))
+
+    def pump(point):
+        for vals in W_EVENTS[point]:
+            code = pick(vals)
+
+            @pl.when(code >= 0)
+            def _():
+                h, c = code // 64, code // 8 % 8
+                w_copy(h, c, 0).wait_recv()
+                for d in range(3):
+                    if any(v >= 0 and v // 2**d % 2 for v in vals):
+                        guard(code // 2**d % 2 == 1)(lambda d=d: w_copy(h, c, d).start())
+
+    for load in own_loads:
+        load.wait()
+    for c in (0, 1):
+        w_own(c, lambda copy: copy.start())
+
+    early = t // 2
+
+    def kv_copy(slot, part, ssem, who):
+        view = kv.at[slot, early + part * (1 - 2 * early)]
+        return push(view, view, ssem, kv_rsem.at[slot, part], {"sp": who})
+
+    def kv_out(part, act):
+        for step in range(levels - 1, 0, -1):
+            guard(z + step < levels)(lambda step=step: act(kv_copy(sp, part, kv_ssem.at[part, step], sp + 2 * step)))
+        guard(y == 0)(lambda: act(kv_copy(sp, part, kv_ssem.at[part, 0], side)))
+
+    def kv_across(part, step, act):
+        guard(z >= step)(lambda: act(kv_copy(sp - 2 * step, part, kv_fsem.at[part, step - 1], side)))
+
+    def kv_pass(part, step):
+        def both(copy):
+            copy.wait_recv()
+            copy.start()
+
+        kv_across(part, step, both)
+
+    def dot(w):
+        return jnp.dot(normed[...], w[...], preferred_element_type=F32)
+
+    def project_kv(groups, pair):
+        for i, g in enumerate(groups):
+            x = (tok_ref[...] if g is None else xall[g]).astype(F32)
+            inverse = lax.rsqrt(jnp.mean(x * x, axis=-1, keepdims=True) + 1e-06)
+            at = rows * (t % 2 if i == 0 else 1 - t % 2)
+            normed[pl.ds(pl.multiple_of(at, rows), rows)] = (x * inverse * gain_ref[...]).astype(BF16)
+        both = dot(wkv).astype(BF16)
+        kv[sp, pair, 0] = both[:, :kv_cols]
+        kv[sp, pair, 1] = both[:, kv_cols:]
+
+    def project_rest(pair, points):
+        at = pl.ds(pl.multiple_of(pair * 2 * rows, 2 * rows), 2 * rows)
+        gate = dot(wc).astype(BF16).astype(F32)
+        pump(points[0])
+        prod_sc[at] = (gate * dot(wu).astype(BF16).astype(F32)).astype(BF16)
+        pump(points[1])
+        q_sc[at] = dot(wq).astype(BF16)
+        pump(points[2])
+        gate_sc[at] = dot(wb).astype(BF16)
+        pump(points[3])
+
+    to_near.wait_recv()
+    for load in loads[:2]:
+        load.wait()
+    project_kv((None, near), early)
+    pl.semaphore_wait(near_by, column)
+    tell_column(further)
+    pl.semaphore_wait(further, column)
+    kv_out(0, lambda copy: copy.start())
+    for c in (2, 3):
+        w_own(c, lambda copy: copy.start())
+    for load in loads[2:]:
+        load.wait()
+    pump(0)
+    project_rest(early, (1, 2, 3, 4))
+    to_far[0].wait_recv()
+    relay[0].start()
+    for step in range(1, levels):
+        kv_pass(0, step)
+    pump(5)
+    to_far[1].wait_recv()
+    relay[1].start()
+    for c in range(2):
+        relay[c].wait_recv()
+    project_kv((far, diag), 1 - early)
+    kv_out(1, lambda copy: copy.start())
+    pump(6)
+    project_rest(1 - early, (7, 8, 9, 10))
+    halo = push(prod_sc.at[pl.ds(toks - HALO, HALO)], prev, halo_sem.at[0], halo_sem.at[1], {"sp": sp + 1})
+    guard(sp < n - 1)(halo.start)
+
+    key_i = lax.broadcasted_iota(jnp.int32, (toks, toks), 0)
+    key_j = lax.broadcasted_iota(jnp.int32, (toks, toks), 1)
+    later = (key_i > key_j).astype(F32).astype(BF16)
+    scale = HEAD_DIM ** (-0.5)
+    order = (t, far, near, diag)
+
+    def visit(slot, masked):
+        for h in range(heads):
+            cols = pl.ds(h * HEAD_DIM, HEAD_DIM)
+            kv_at = pl.ds((h // grouping) * HEAD_DIM, HEAD_DIM)
+            keys = kv[slot, :, 0, :, kv_at].reshape(toks, HEAD_DIM)
+            vals = kv[slot, :, 1, :, kv_at].reshape(toks, HEAD_DIM)
+            s = lax.dot_general(q_sc[:, cols], keys, NT, preferred_element_type=F32) * scale + shift_ref[0, h]
+            soft = softplus(s)
+            if masked:
+                soft = jnp.where(key_j < key_i, soft, 0.0)
+            high = soft.astype(BF16)
+            low = (soft - high.astype(F32)).astype(BF16)
+            after = jnp.dot(high, later, preferred_element_type=F32) + jnp.dot(low, later, preferred_element_type=F32)
+            weight = jnp.exp(s - soft - after)
+            if masked:
+                weight = jnp.where(key_j < key_i, weight, 0.0)
+            part = jnp.dot(weight.astype(BF16), vals, preferred_element_type=F32)
+            total = jnp.broadcast_to(after[:, 0:1] + soft[:, 0:1], (toks, HEAD_DIM))
+            if masked:
+                acc[:, cols] = part
+                suffix[h] = total
+            else:
+                acc[:, cols] += jnp.exp(-suffix[h]) * part
+                suffix[h] += total
+
+    def convolve():
+        @pl.when(sp == 0)
+        def _():
+            prev[...] = jnp.zeros(prev.shape, BF16)
+
+        guard(sp > 0)(halo.wait_recv)
+        ext[pl.ds(HALO, toks)] = prod_sc[...].astype(F32)
+        ext[pl.ds(0, HALO)] = prev[...].astype(F32)
+        summed = jnp.zeros((toks, ext.shape[1]), F32)
+        for tap in range(CONV_K):
+            summed = summed + taps_ref[tap : tap + 1, :] * ext[pl.ds(HALO - (CONV_K - 1) + tap, toks)]
+        ext[pl.ds(HALO, toks)] = gate_sc[...].astype(F32) * summed
+        for i, g in enumerate(order):
+            conv[pl.ds(i * rows, rows)] = ext[pl.ds(pl.multiple_of(HALO + g * rows, HALO), rows)].astype(BF16)
+
+    def act_copy(i):
+        return push((attn, conv)[i], guest.at[i], act_sem.at[0, i], act_sem.at[1, i], {"sp": host})
+
+    for step in range(1, levels):
+        kv_pass(1, step)
+    visit(sp, True)
+    pump(11)
+    convolve()
+    guard(outer)(lambda: act_copy(1).start())
+    pump(12)
+    for i in range(1, n):
+        slot = sp - i
+
+        @pl.when(slot >= 0)
+        def _():
+            def take(part):
+                kv_copy(slot, part, kv_ssem.at[part, 0], side).wait_recv()
+
+            if i % 2 == 1:
+                take(0)
+                take(1)
+            visit(slot, False)
+
+        pump(12 + i)
+
+    for h in range(heads):
+        spread = suffix[h].T[0:1, :]
+        logw_ref[h : h + 1, :] = jnp.log(jnp.maximum(1.0 - jnp.exp(-spread), 0.05))
+    for i, g in enumerate(order):
+        attn[pl.ds(i * rows, rows)] = acc[pl.ds(pl.multiple_of(g * rows, rows), rows)].astype(BF16)
+    guard(outer)(lambda: act_copy(0).start())
+
+    def d2d_copy(i):
+        return push(snd.at[i], d2d.at[i], d2d_sem.at[0, i], d2d_sem.at[1, i], {"tp": near})
+
+    def x_copy(i):
+        return push(xsnd.at[i], xrcv.at[i], x_sem.at[0, i], x_sem.at[1, i], {"tp": far})
+
+    def ret_copy(r):
+        return push(gsnd.at[r], grcv.at[r], ret_sem.at[0, r], ret_sem.at[1, r], {"sp": host})
+
+    def put(h, block):
+        out_ref[:, pl.ds(pl.multiple_of(h * feats, feats), feats)] = block
+
+    def active(i):
+        vals = CELLS[i]
+        if all(v >= 0 for v in vals):
+            return lambda body: body()
+        return pl.when(pick(vals) >= 0)
+
+    own_cells = n
+
+    def first(i):
+        @active(i)
+        def _():
+            j = pick(CELLS[i])
+            a, b = (attn, conv) if i < own_cells else (guest.at[0], guest.at[1])
+            share = lax.dot_general(a[...], wo[j, 0], NT, preferred_element_type=F32)
+            share = (share + lax.dot_general(b[...], wo[j, 1], NT, preferred_element_type=F32)).astype(BF16)
+            snd[i] = share[2 * rows :]
+            keep[i] = share[: 2 * rows]
+            d2d_copy(i).start()
+
+    def second(i):
+        @active(i)
+        def _():
+            d2d_copy(i).wait_recv()
+            xsnd[i] = (keep[i, pl.ds(rows, rows)].astype(F32) + d2d[i, pl.ds(rows, rows)].astype(F32)).astype(BF16)
+            x_copy(i).start()
+
+    def third(i):
+        @active(i)
+        def _():
+            x_copy(i).wait_recv()
+            own = keep[i, pl.ds(0, rows)].astype(F32) + d2d[i, pl.ds(0, rows)].astype(F32)
+            done = (own + xrcv[i].astype(F32)).astype(BF16)
+            if i < own_cells:
+                put(pick(CELLS[i]), done)
+            else:
+                gsnd[i - own_cells] = done
+                ret_copy(i - own_cells).start()
+
+    done_first = []
+    for step, i in enumerate(CELL_ORDER):
+        pump(20 + step)
+        if i == own_cells:
+            @pl.when(inner)
+            def _():
+                act_copy(1).wait_recv()
+                act_copy(0).wait_recv()
+
+        first(i)
+        done_first.append(i)
+        if step >= 1:
+            second(done_first[step - 1])
+        if step >= 3:
+            third(done_first[step - 3])
+    second(done_first[-1])
+    for i in done_first[-3:]:
+        third(i)
+    for r in range(len(CELLS) - own_cells):
+        @pl.when(outer)
+        def _():
+            ret_copy(r).wait_recv()
+            put(pick(CELL_BACK[r]), grcv[r])
+
+    for copy in (*to_far, to_near, *relay):
+        copy.wait_send()
+    guard(sp < n - 1)(halo.wait_send)
+    for part in range(2):
+        kv_out(part, lambda copy: copy.wait_send())
+        for step in range(1, levels):
+            kv_across(part, step, lambda copy: copy.wait_send())
+    for c in range(4):
+        w_own(c, lambda copy: copy.wait_send())
+    for slots in W_EVENTS:
+        for vals in slots:
+            w_spread(vals, lambda copy: copy.wait_send())
+
+    @pl.when(outer)
+    def _():
+        for i in range(2):
+            act_copy(i).wait_send()
+
+    for i in range(len(CELLS)):
+        @active(i)
+        def _():
+            d2d_copy(i).wait_send()
+            x_copy(i).wait_send()
+            if i >= own_cells:
+                ret_copy(i - own_cells).wait_send()
+
+
+def grid_local(
+    n, tokens, norm_gain, w_query, w_key, w_value, score_shift, w_conv_b, w_conv_c, w_conv_u,
+    conv_kernel, w_out_att, w_out_conv,
+):
+    rows, d = tokens.shape
+    toks = 4 * rows
+    feats, att_cols = w_out_att.shape
+    conv_cols = w_out_conv.shape[1]
+    heads = score_shift.shape[0]
+    kv_cols = w_key.shape[1]
+    cells = len(CELLS)
+    guests = cells - n
+    vmem = pl.BlockSpec(memory_space=pltpu.VMEM)
+    smem = pl.BlockSpec(memory_space=pltpu.SMEM)
+    hbm = pl.BlockSpec(memory_space=pl.ANY)
+    dma = pltpu.SemaphoreType.DMA
+    regular = pltpu.SemaphoreType.REGULAR
+    out, logw = pl.pallas_call(
+        functools.partial(grid_kernel, n),
+        out_shape=(
+            jax.ShapeDtypeStruct((rows, n * feats), BF16),
+            jax.ShapeDtypeStruct((heads, toks), F32),
+        ),
+        in_specs=[vmem, vmem, hbm, hbm, hbm, smem, hbm, hbm, hbm, vmem, hbm, hbm],
+        out_specs=(vmem, vmem),
+        scratch_shapes=[
+            pltpu.VMEM(w_query.shape, BF16),
+            pltpu.VMEM((d, 2 * kv_cols), BF16),
+            *[pltpu.VMEM(w.shape, BF16) for w in (w_conv_b, w_conv_c, w_conv_u)],
+            pltpu.VMEM((4, rows, d), BF16),
+            pltpu.VMEM((2 * rows, d), BF16),
+            pltpu.VMEM((toks, w_query.shape[1]), BF16),
+            pltpu.VMEM((n, 2, 2, 2 * rows, kv_cols), BF16),
+            pltpu.VMEM((n, 2, feats, att_cols), BF16),
+            pltpu.VMEM((toks, conv_cols), BF16),
+            pltpu.VMEM((toks, conv_cols), BF16),
+            pltpu.VMEM((HALO, conv_cols), BF16),
+            pltpu.VMEM((toks + HALO, conv_cols), F32),
+            pltpu.VMEM((toks, att_cols), BF16),
+            pltpu.VMEM((toks, conv_cols), BF16),
+            pltpu.VMEM((toks, att_cols), F32),
+            pltpu.VMEM((heads, toks, HEAD_DIM), F32),
+            *[pltpu.VMEM((cells, 2 * rows, feats), BF16)] * 3,
+            *[pltpu.VMEM((cells, rows, feats), BF16)] * 2,
+            pltpu.VMEM((2, toks, att_cols), BF16),
+            *[pltpu.VMEM((guests, rows, feats), BF16)] * 2,
+            dma((8,)), dma((5,)), dma((5,)), dma((2, n // 2)), dma((2, n // 2 - 1)), dma((n, 2)), dma((3, n, 4)), dma((n, 4)),
+            dma((2,)), dma((2, cells)), dma((2, cells)), dma((2, 2)), dma((2, guests)), regular, regular,
+        ],
+        compiler_params=pltpu.CompilerParams(
+            collective_id=0, has_side_effects=True, vmem_limit_bytes=60 * 1024 * 1024
+        ),
+    )(
+        tokens, norm_gain.reshape(1, d), w_query, w_key, w_value, score_shift.reshape(1, heads),
+        w_conv_b, w_conv_c, w_conv_u, conv_kernel, w_out_att, w_out_conv,
+    )
+    return (out, logw.T)
+
 
 def solution(mesh):
+    n = mesh.shape["sp"]
+    body = grid_local if n == len(W_OWN[0]) and mesh.shape["tp"] == 4 else local
     return jax.shard_map(
-        functools.partial(local, mesh.shape["sp"]),
+        functools.partial(body, n),
         mesh=mesh,
         in_specs=(
             P(("sp", "tp"), None), P(), P(None, "tp"), P(None, "tp"), P(None, "tp"), P("tp"),

time: 71.8 us -> 76.2 us (1.061)
  the two profiles are of different devices: /device:TPU:9 before, /device:TPU:28 now
where the time goes in v1:
time: 76.2 us; the launch traced here: 76 us
  Pallas kernels  72.2 us (95%)
  local copies, waits for them, and re-layouts  3.12 us (4%)
    pallas_call x1, Pallas kernels, grid_local(): pl.pallas_call(functools.partial(grid_kernel, n), out_shape=(jax.ShapeDty...  72.2 us
    unnamed x2, local copies, waits for them, and re-layouts  3.12 us

profile of v1, /device:TPU:28, one launch (start us, length us, event | category | flops | bytes accessed | tf_op | source)
XLA Modules:
  0.0 76.0 jit_solution(2589892390343129624)
XLA Ops:
  0.6 72.2 %shard_map.131 = (bf16[64,4096]{1,0:T(8,128)(2,1)}, f32[2,256]{1,0:T(2,128)}) custom-call(bf16[64,4096]{1,0:T(8,128)(2,1)} %tok_ref.1, f32[1,4096]{1,0:T(1,128)} %bitcast.3, bf16[4096,256]{1,0:T(8,128)(2,1)} %wq_hbm.1, bf16[4096,128]{1,0:T(8,128)(2,1)} %wk_hbm.1, bf16[4096,128]{1,0:T(8,128)(2,1)} %wv_hbm.1, f32[1,2]{1,0:T(1,128)} %bitcast.5, ...), custom_call_target="tpu_custom_call" | custom-call | tf_op jit(solution)/shard_map/pallas_call | solution.py:848
  72.9 1.9 %copy.16 = bf16[64,4096]{1,0:T(8,128)(2,1)} copy(bf16[64,4096]{1,0:T(8,128)(2,1)} %get-tuple-element.8) | data formatting | bytes 1048576
  74.7 1.3 %copy.17 = f32[256,2]{0,1:T(2,128)} copy(f32[256,2]{0,1:T(2,128)} %bitcast.4) | data formatting | bytes 4096

commit v2 on v1

--- a/solution.py
+++ b/solution.py
@@ -14,69 +14,91 @@
 BF16 = jnp.bfloat16
 MESH = pl.DeviceIdType.MESH
 NT = (((1,), (1,)), ((), ()))
-W_OWN = [(5, 1, 6, 7, 7, 3, 6, 2), (5, 5, 4, 7, 3, 3, 6, 6), (5, 5, 7, 7, 7, 5, 6, 6), (5, 5, 7, 6, 3, 7, 6, 6)]
-W_EVENTS = [[],
+EVENTS = [[(10, 138, 270, 398, 526, 646, 780, 908), (-1, -1, -1, -1, -1, 664, -1, -1)],
+ [(74, 194, 330, 450, 586, 706, 840, 924),
+  (26, 154, 278, 414, 542, 662, 796, -1),
+  (-1, -1, 296, -1, -1, 680, -1, -1)],
  [],
- [(73, 1, 1, 68, 386, 193, 260, 324), (132, 192, 195, 129, -1, 258, 458, 386), (-1, -1, 256, 326, -1, 454, -1, -1)],
+ [(-1, 168, 292, 428, 548, 692, 804, 940)],
+ [(-1, -1, -1, -1, -1, 393, -1, -1)],
+ [(42, 162, 290, 418, 554, 674, 808, -1), (-1, -1, 312, -1, -1, -1, -1, -1)],
+ [(-1, 184, 75, 203, 331, 459, 585, 713), (-1, -1, 308, 436, 564, 517, 820, 948)],
+ [(58, 178, 306, 440, 562, 409, 824, 952),
+  (-1, 393, 517, 434, 265, 690, 901, 773),
+  (-1, -1, 553, 645, 773, 901, -1, 649)],
+ [(90, 210, 346, 466, 75, 203, 329, 457),
+  (131, 3, 405, 648, 602, 722, 856, 789),
+  (265, 425, -1, 661, 677, 917, 917, -1)],
  [],
+ [(-1, 441, 533, 293, 789, 933, 537, 665), (-1, -1, -1, -1, -1, 425, 933, 805)],
+ [(147, 19, 3, 131, -1, -1, -1, -1), (281, -1, -1, -1, -1, -1, -1, -1)],
+ [(-1, -1, 569, 664, -1, -1, -1, -1)],
+ [(-1, -1, 91, 219, 347, 475, 73, 201)],
+ [(313, 649, 19, 147, 805, 773, -1, -1), (-1, -1, 548, 693, -1, -1, -1, -1)],
+ [(-1, 65, 57, 321, 258, 577, 601, 729),
+  (-1, 81, 35, 337, 281, 593, 345, 833),
+  (-1, -1, 564, -1, 821, -1, 949, 849),
+  (-1, -1, 681, -1, 449, -1, 553, -1),
+  (-1, -1, 193, -1, 465, -1, 645, -1),
+  (-1, -1, 209, -1, -1, -1, 705, -1),
+  (-1, -1, -1, -1, -1, -1, 721, -1)],
+ [(-1, -1, 676, 696, 91, 386, 569, -1), (-1, -1, -1, -1, 274, 441, -1, -1), (-1, -1, -1, -1, 297, -1, -1, -1)],
+ [(-1, -1, -1, 517, 917, 789, 89, 473),
+  (-1, -1, -1, 163, 290, 321, 449, 821),
+  (-1, -1, -1, 905, 313, 337, 465, 681),
+  (-1, -1, -1, 65, 193, -1, -1, 577),
+  (-1, -1, -1, 81, 209, -1, -1, 593)],
+ [(-1, -1, -1, -1, -1, 219, -1, 697), (-1, -1, -1, -1, -1, 514, -1, -1), (-1, -1, -1, -1, -1, 137, -1, -1)],
+ [(-1, -1, -1, -1, -1, 805, 297, 217),
+  (-1, -1, -1, -1, -1, 402, 193, 321),
+  (-1, -1, -1, -1, -1, 65, 209, 337),
+  (-1, -1, -1, -1, -1, 81, -1, -1)],
  [],
- [(81, 9, 8, 73, 394, 205, 268, 332),
-  (148, 204, 200, 139, 338, 458, -1, 394),
-  (89, 212, 270, 334, -1, -1, -1, -1),
-  (156, -1, 278, 350, -1, -1, -1, -1)],
- [(192, 17, 208, 144, 402, 272, 466, 340),
-  (200, 216, 286, 258, 149, 466, 276, -1),
-  (-1, 24, 16, 80, 344, -1, 474, -1),
-  (-1, -1, 219, -1, -1, -1, -1, -1)],
- [],
- [(208, 324, 384, 152, 410, 209, -1, 402), (268, -1, -1, 452, 157, 474, -1, -1), (-1, -1, -1, -1, 449, -1, -1, -1)],
- [(-1, 128, 28, 88, -1, -1, 284, 348), (-1, -1, 67, -1, -1, -1, -1, -1)],
- [(-1, -1, -1, -1, -1, -1, 322, -1)],
- [(276, 140, 392, 264, 456, 145, -1, 410), (-1, -1, -1, 460, 4, 133, -1, -1), (-1, -1, -1, -1, 200, 386, -1, -1)],
- [(-1, 144, 72, 0, -1, -1, 144, 192), (-1, -1, 320, -1, -1, -1, 330, -1)],
- [(-1, 332, 338, 272, 466, 76, -1, 256), (-1, -1, -1, 464, -1, 394, -1, -1)],
- [(-1, -1, -1, -1, 193, -1, -1, -1)],
- [(-1, -1, -1, 9, -1, -1, -1, 204)],
- [(-1, -1, -1, -1, 129, 141, -1, 266)],
- [(-1, -1, -1, -1, -1, 152, -1, -1)],
- [],
- [],
- [(320, -1, 81, -1, -1, -1, 156, -1), (-1, -1, 328, -1, -1, -1, 336, -1)],
- [(280, -1, -1, 282, -1, -1, -1, -1), (136, -1, -1, 472, -1, -1, -1, -1)],
- [(216, 152, -1, -1, 474, 402, 448, -1)],
- [(328, -1, 400, 17, 72, 0, 344, 212),
-  (64, -1, -1, -1, 320, 408, -1, 144),
-  (-1, -1, -1, -1, 136, -1, -1, 272),
-  (-1, -1, -1, -1, 221, -1, -1, 128),
-  (-1, -1, -1, -1, -1, -1, -1, 282)],
- [(344, 348, 89, -1, 328, 264, 192, 140),
-  (340, 260, 344, -1, -1, 12, 200, 152),
-  (-1, 264, -1, -1, -1, 216, 128, -1),
-  (-1, 272, -1, -1, -1, -1, 210, -1),
-  (-1, 280, -1, -1, -1, -1, 220, -1)],
- [(256, 337, -1, 384, 68, 20, 136, 216),
-  (-1, -1, -1, 25, 84, 64, -1, -1),
-  (-1, -1, -1, 392, 8, 28, -1, -1),
-  (-1, -1, -1, -1, 92, -1, -1, -1)],
- [(-1, -1, 412, 400, 16, 280, -1, -1), (-1, -1, -1, 408, 208, -1, -1, -1)],
- [(-1, -1, 448, 336, 24, 80, -1, -1),
-  (-1, -1, 464, -1, -1, 88, -1, -1),
-  (-1, -1, 456, -1, -1, -1, -1, -1),
-  (-1, -1, 472, -1, -1, -1, -1, -1)],
- [],
+ [(-1, -1, -1, -1, -1, -1, -1, 393),
+  (-1, -1, -1, -1, -1, -1, -1, 565),
+  (-1, -1, -1, -1, -1, -1, -1, 65),
+  (-1, -1, -1, -1, -1, -1, -1, 81)],
+ [(-1, -1, 50, 179, 403, 277, -1, 425), (-1, -1, -1, 549, 9, -1, -1, -1), (-1, -1, -1, -1, 949, -1, -1, -1)],
+ [(161, 401, -1, 937, -1, 418, -1, -1), (177, -1, -1, -1, -1, 169, -1, -1), (-1, -1, -1, -1, -1, 945, -1, -1)],
+ [(289, 665, 147, 19, -1, -1, 313, -1), (-1, 33, -1, 673, -1, -1, 513, -1), (-1, 49, -1, -1, -1, -1, -1, -1)],
+ [(385, 34, 825, 35, 306, 817, 657, 513),
+  (401, 697, 385, 1, 385, -1, 673, 529),
+  (417, 257, 417, 49, 417, -1, 689, 545),
+  (433, 273, 433, -1, 433, -1, -1, -1),
+  (-1, 289, -1, -1, -1, -1, -1, -1),
+  (-1, 305, -1, -1, -1, -1, -1, -1)],
+ [(162, 531, 691, 769, 434, 259, 441, 257),
+  (537, 513, 769, 785, 57, 185, 257, 273),
+  (178, 545, 785, 801, 897, 145, 273, 289),
+  (569, 561, 801, 817, 929, -1, -1, 305),
+  (513, -1, -1, -1, -1, -1, -1, -1),
+  (545, -1, -1, -1, -1, -1, -1, -1)],
+ [(681, 673, 641, -1, 17, 274, 385, 401),
+  (641, -1, 657, -1, 33, 289, 401, 433),
+  (657, -1, -1, -1, -1, 305, 417, -1),
+  (689, -1, -1, -1, -1, -1, -1, -1)],
+ [(-1, -1, 953, 257, 641, 529, -1, -1),
+  (-1, -1, 897, 273, 657, 545, -1, -1),
+  (-1, -1, 913, 305, 689, 561, -1, -1),
+  (-1, -1, 929, -1, -1, -1, -1, -1)],
+ [(-1, -1, -1, 529, 129, 1, -1, -1),
+  (-1, -1, -1, 561, 145, 17, -1, -1),
+  (-1, -1, -1, -1, 161, 33, -1, -1),
+  (-1, -1, -1, -1, 177, 49, -1, -1)],
+ [(-1, -1, -1, 913, -1, -1, -1, -1), (-1, -1, -1, 945, -1, -1, -1, -1)],
+ [(-1, -1, 129, -1, -1, -1, -1, -1), (-1, -1, 161, -1, -1, -1, -1, -1), (-1, -1, 177, -1, -1, -1, -1, -1)],
  []]
 CELLS = [(0, 1, 2, 3, 4, 5, 6, 7),
- (2, 3, 4, 2, 6, 7, 4, 5),
- (3, 0, 3, 1, 7, 2, 7, 6),
- (1, 2, 0, 4, 2, 6, 5, 4),
- (5, 4, 1, 7, 5, 3, 3, 2),
- (4, 5, 5, 0, 1, 0, 2, 3),
- (-1, -1, 6, 6, 3, 4, -1, -1),
- (-1, -1, 7, 5, 0, 1, -1, -1),
- (-1, -1, 6, 6, 0, 0, -1, -1),
- (-1, -1, 7, 7, 1, 1, -1, -1)]
+ (1, 3, 4, 1, 6, 7, 7, 5),
+ (2, 0, 0, 5, 2, 3, 4, 6),
+ (3, 2, 3, 0, 3, 6, 5, 4),
+ (4, 4, 14, 14, 7, 1, 2, 2),
+ (5, 5, 5, 6, 0, 2, 3, 3),
+ (-1, -1, 23, 2, 5, 4, -1, -1),
+ (-1, -1, 6, 4, 1, 0, -1, -1),
+ (-1, -1, 7, 23, 8, 8, -1, -1),
+ (-1, -1, 1, 7, 17, 17, -1, -1)]
 CELL_BACK = [(6, 6, -1, -1, -1, -1, 0, 0), (7, 7, -1, -1, -1, -1, 1, 1)]
-CELL_ORDER = (0, 1, 2, 3, 4, 5, 6, 7, 8, 9)
 
 
 def softplus(z):
@@ -452,10 +474,10 @@
     n,
     tok_ref, gain_ref, wq_hbm, wk_hbm, wv_hbm, shift_ref, wb_hbm, wc_hbm, wu_hbm, taps_ref, woa_ref, woc_ref,
     out_ref, logw_ref,
-    wq, wkv, wb, wc, wu, xall, normed, q_sc, kv, wo, gate_sc, prod_sc, prev, ext, attn, conv, acc, suffix,
-    snd, keep, d2d, xsnd, xrcv, guest, gsnd, grcv,
-    load_sem, tok_ssem, tok_rsem, kv_ssem, kv_fsem, kv_rsem, w_ssem, w_rsem, halo_sem, d2d_sem, x_sem,
-    act_sem, ret_sem, near_by, further,
+    wq, wkv, wb, wc, wu, xall, normed, q_sc, kv, wo, gate_sc, prod_sc, prev, ext, acts, acc, suffix,
+    snd, keep, d2d, xsnd, xrcv, gsnd, grcv,
+    load_sem, tok_ssem, tok_rsem, kv_ssem, kv_rsem, w_ssem, w_rsem, halo_sem, d2d_sem, x_sem,
+    act_sem, ret_sem, near_by,
 ):
     sp = lax.axis_index("sp")
     t = lax.axis_index("tp")
@@ -470,7 +492,6 @@
     levels = n // 2
     has_up, has_down = z < levels - 1, z > 0
     outer = jnp.logical_or(z == 0, z == levels - 1)
-    inner = jnp.logical_and(z > 0, z < levels - 1)
     rows = tok_ref.shape[0]
     toks = 4 * rows
     half = rows // 2
@@ -539,61 +560,41 @@
     to_near.start()
     tell_column(near_by)
 
+    early = t // 2
+
     def w_copy(h, c, d):
         view = wo.at[h, c // 2, pl.ds(pl.multiple_of((c % 2) * fpart, fpart), fpart)]
         return push(view, view, w_ssem.at[d, h, c], w_rsem.at[h, c], {"sp": ways[d]})
 
-    def w_spread(vals, act):
+    def kv_copy(h, c, d):
+        view = kv.at[h, early + (c - 4) * (1 - 2 * early)]
+        return push(view, view, kv_ssem.at[d, h, c - 4], kv_rsem.at[h, c - 4], {"sp": ways[d]})
+
+    def event(vals, arrive, leave):
         code = pick(vals)
-        for d in range(3):
-            if any(v >= 0 and v // 2**d % 2 for v in vals):
-                guard(jnp.logical_and(code >= 0, code // 2**d % 2 == 1))(
-                    lambda d=d: act(w_copy(code // 64, code // 8 % 8, d))
-                )
-
-    def w_own(c, act):
-        mask = pick(W_OWN[c])
-        for d in range(3):
-            if any(v // 2**d % 2 for v in W_OWN[c]):
-                guard(mask // 2**d % 2 == 1)(lambda d=d: act(w_copy(sp, c, d)))
+        h, c = code // 128, code // 16 % 8
+        for copy_of, low, high in ((w_copy, 0, 4), (kv_copy, 4, 6)):
+            mine = [v for v in vals if v >= 0 and low <= v // 16 % 8 < high]
+            if not mine:
+                continue
+            live = jnp.logical_and(code >= 16 * low, c < high) if low == 0 else c >= low
+            live = jnp.logical_and(live, code >= 0)
+
+            @pl.when(live)
+            def _():
+                if arrive and any(v % 2 for v in mine):
+                    pl.when(code % 2 == 1)(lambda: copy_of(h, c, 0).wait_recv())
+                for d in range(3):
+                    if any(v // 2 // 2**d % 2 for v in mine):
+                        pl.when(code // 2 // 2**d % 2 == 1)(lambda d=d: leave(copy_of(h, c, d)))
 
     def pump(point):
-        for vals in W_EVENTS[point]:
-            code = pick(vals)
-
-            @pl.when(code >= 0)
-            def _():
-                h, c = code // 64, code // 8 % 8
-                w_copy(h, c, 0).wait_recv()
-                for d in range(3):
-                    if any(v >= 0 and v // 2**d % 2 for v in vals):
-                        guard(code // 2**d % 2 == 1)(lambda d=d: w_copy(h, c, d).start())
+        for vals in EVENTS[point]:
+            event(vals, True, lambda copy: copy.start())
 
     for load in own_loads:
         load.wait()
-    for c in (0, 1):
-        w_own(c, lambda copy: copy.start())
-
-    early = t // 2
-
-    def kv_copy(slot, part, ssem, who):
-        view = kv.at[slot, early + part * (1 - 2 * early)]
-        return push(view, view, ssem, kv_rsem.at[slot, part], {"sp": who})
-
-    def kv_out(part, act):
-        for step in range(levels - 1, 0, -1):
-            guard(z + step < levels)(lambda step=step: act(kv_copy(sp, part, kv_ssem.at[part, step], sp + 2 * step)))
-        guard(y == 0)(lambda: act(kv_copy(sp, part, kv_ssem.at[part, 0], side)))
-
-    def kv_across(part, step, act):
-        guard(z >= step)(lambda: act(kv_copy(sp - 2 * step, part, kv_fsem.at[part, step - 1], side)))
-
-    def kv_pass(part, step):
-        def both(copy):
-            copy.wait_recv()
-            copy.start()
-
-        kv_across(part, step, both)
+    pump(0)
 
     def dot(w):
         return jnp.dot(normed[...], w[...], preferred_element_type=F32)
@@ -623,29 +624,22 @@
     for load in loads[:2]:
         load.wait()
     project_kv((None, near), early)
-    pl.semaphore_wait(near_by, column)
-    tell_column(further)
-    pl.semaphore_wait(further, column)
-    kv_out(0, lambda copy: copy.start())
-    for c in (2, 3):
-        w_own(c, lambda copy: copy.start())
+    pump(1)
     for load in loads[2:]:
         load.wait()
-    pump(0)
-    project_rest(early, (1, 2, 3, 4))
+    project_rest(early, (2, 3, 4, 5))
+    pump(6)
     to_far[0].wait_recv()
     relay[0].start()
-    for step in range(1, levels):
-        kv_pass(0, step)
-    pump(5)
+    pump(7)
     to_far[1].wait_recv()
     relay[1].start()
     for c in range(2):
         relay[c].wait_recv()
     project_kv((far, diag), 1 - early)
-    kv_out(1, lambda copy: copy.start())
-    pump(6)
-    project_rest(1 - early, (7, 8, 9, 10))
+    pump(8)
+    project_rest(1 - early, (9, 10, 11, 12))
+    pl.semaphore_wait(near_by, column)
     halo = push(prod_sc.at[pl.ds(toks - HALO, HALO)], prev, halo_sem.at[0], halo_sem.at[1], {"sp": sp + 1})
     guard(sp < n - 1)(halo.start)
 
@@ -693,38 +687,28 @@
             summed = summed + taps_ref[tap : tap + 1, :] * ext[pl.ds(HALO - (CONV_K - 1) + tap, toks)]
         ext[pl.ds(HALO, toks)] = gate_sc[...].astype(F32) * summed
         for i, g in enumerate(order):
-            conv[pl.ds(i * rows, rows)] = ext[pl.ds(pl.multiple_of(HALO + g * rows, HALO), rows)].astype(BF16)
+            acts[0, 1, pl.ds(i * rows, rows)] = ext[pl.ds(pl.multiple_of(HALO + g * rows, HALO), rows)].astype(BF16)
 
     def act_copy(i):
-        return push((attn, conv)[i], guest.at[i], act_sem.at[0, i], act_sem.at[1, i], {"sp": host})
-
-    for step in range(1, levels):
-        kv_pass(1, step)
+        return push(acts.at[0, i], acts.at[1, i], act_sem.at[0, i], act_sem.at[1, i], {"sp": host})
+
     visit(sp, True)
-    pump(11)
+    pump(13)
     convolve()
     guard(outer)(lambda: act_copy(1).start())
-    pump(12)
+    pump(14)
     for i in range(1, n):
-        slot = sp - i
-
-        @pl.when(slot >= 0)
+        pump(14 + i)
+
+        @pl.when(sp >= i)
         def _():
-            def take(part):
-                kv_copy(slot, part, kv_ssem.at[part, 0], side).wait_recv()
-
-            if i % 2 == 1:
-                take(0)
-                take(1)
-            visit(slot, False)
-
-        pump(12 + i)
+            visit(sp - i, False)
 
     for h in range(heads):
         spread = suffix[h].T[0:1, :]
         logw_ref[h : h + 1, :] = jnp.log(jnp.maximum(1.0 - jnp.exp(-spread), 0.05))
     for i, g in enumerate(order):
-        attn[pl.ds(i * rows, rows)] = acc[pl.ds(pl.multiple_of(g * rows, rows), rows)].astype(BF16)
+        acts[0, 0, pl.ds(i * rows, rows)] = acc[pl.ds(pl.multiple_of(g * rows, rows), rows)].astype(BF16)
     guard(outer)(lambda: act_copy(0).start())
 
     def d2d_copy(i):
@@ -745,13 +729,35 @@
             return lambda body: body()
         return pl.when(pick(vals) >= 0)
 
-    own_cells = n
+    def kinds(i, own, guest):
+        code = pick(CELLS[i])
+        if all(v < n for v in CELLS[i]):
+            own(code)
+        else:
+            if any(0 <= v < n for v in CELLS[i]):
+                pl.when(code < n)(lambda: own(code))
+            pl.when(code >= n)(lambda: guest(code % n, code // n - 1))
 
     def first(i):
         @active(i)
         def _():
-            j = pick(CELLS[i])
-            a, b = (attn, conv) if i < own_cells else (guest.at[0], guest.at[1])
+            def own(j):
+                return None
+
+            def visitor(j, r):
+                @pl.when(r == 0)
+                def _():
+                    act_copy(1).wait_recv()
+                    act_copy(0).wait_recv()
+
+            kinds(i, own, visitor)
+            code = pick(CELLS[i])
+            j = code % n
+            if all(v < n for v in CELLS[i]):
+                a, b = acts.at[0, 0], acts.at[0, 1]
+            else:
+                who = jnp.minimum(code // n, 1)
+                a, b = acts.at[who, 0], acts.at[who, 1]
             share = lax.dot_general(a[...], wo[j, 0], NT, preferred_element_type=F32)
             share = (share + lax.dot_general(b[...], wo[j, 1], NT, preferred_element_type=F32)).astype(BF16)
             snd[i] = share[2 * rows :]
@@ -771,32 +777,27 @@
             x_copy(i).wait_recv()
             own = keep[i, pl.ds(0, rows)].astype(F32) + d2d[i, pl.ds(0, rows)].astype(F32)
             done = (own + xrcv[i].astype(F32)).astype(BF16)
-            if i < own_cells:
-                put(pick(CELLS[i]), done)
-            else:
-                gsnd[i - own_cells] = done
-                ret_copy(i - own_cells).start()
-
-    done_first = []
-    for step, i in enumerate(CELL_ORDER):
-        pump(20 + step)
-        if i == own_cells:
-            @pl.when(inner)
-            def _():
-                act_copy(1).wait_recv()
-                act_copy(0).wait_recv()
-
+
+            def visitor(j, r):
+                gsnd[r] = done
+                ret_copy(r).start()
+
+            kinds(i, lambda j: put(j, done), visitor)
+
+    steps = len(CELLS)
+    for i in range(steps):
+        pump(22 + i)
         first(i)
-        done_first.append(i)
-        if step >= 1:
-            second(done_first[step - 1])
-        if step >= 3:
-            third(done_first[step - 3])
-    second(done_first[-1])
-    for i in done_first[-3:]:
+        if i >= 1:
+            second(i - 1)
+        if i >= 3:
+            third(i - 3)
+    second(steps - 1)
+    for i in range(steps - 3, steps):
         third(i)
-    for r in range(len(CELLS) - own_cells):
-        @pl.when(outer)
+    pump(22 + steps)
+    for r in range(len(CELL_BACK)):
+        @pl.when(pick(CELL_BACK[r]) >= 0)
         def _():
             ret_copy(r).wait_recv()
             put(pick(CELL_BACK[r]), grcv[r])
@@ -804,28 +805,21 @@
     for copy in (*to_far, to_near, *relay):
         copy.wait_send()
     guard(sp < n - 1)(halo.wait_send)
-    for part in range(2):
-        kv_out(part, lambda copy: copy.wait_send())
-        for step in range(1, levels):
-            kv_across(part, step, lambda copy: copy.wait_send())
-    for c in range(4):
-        w_own(c, lambda copy: copy.wait_send())
-    for slots in W_EVENTS:
+    for slots in EVENTS:
         for vals in slots:
-            w_spread(vals, lambda copy: copy.wait_send())
+            event(vals, False, lambda copy: copy.wait_send())
 
     @pl.when(outer)
     def _():
         for i in range(2):
             act_copy(i).wait_send()
 
-    for i in range(len(CELLS)):
+    for i in range(steps):
         @active(i)
         def _():
             d2d_copy(i).wait_send()
             x_copy(i).wait_send()
-            if i >= own_cells:
-                ret_copy(i - own_cells).wait_send()
+            kinds(i, lambda j: None, lambda j, r: ret_copy(r).wait_send())
 
 
 def grid_local(
@@ -839,7 +833,7 @@
     heads = score_shift.shape[0]
     kv_cols = w_key.shape[1]
     cells = len(CELLS)
-    guests = cells - n
+    guests = len(CELL_BACK)
     vmem = pl.BlockSpec(memory_space=pltpu.VMEM)
     smem = pl.BlockSpec(memory_space=pltpu.SMEM)
     hbm = pl.BlockSpec(memory_space=pl.ANY)
@@ -866,16 +860,14 @@
             pltpu.VMEM((toks, conv_cols), BF16),
             pltpu.VMEM((HALO, conv_cols), BF16),
             pltpu.VMEM((toks + HALO, conv_cols), F32),
-            pltpu.VMEM((toks, att_cols), BF16),
-            pltpu.VMEM((toks, conv_cols), BF16),
+            pltpu.VMEM((2, 2, toks, att_cols), BF16),
             pltpu.VMEM((toks, att_cols), F32),
             pltpu.VMEM((heads, toks, HEAD_DIM), F32),
             *[pltpu.VMEM((cells, 2 * rows, feats), BF16)] * 3,
             *[pltpu.VMEM((cells, rows, feats), BF16)] * 2,
-            pltpu.VMEM((2, toks, att_cols), BF16),
             *[pltpu.VMEM((guests, rows, feats), BF16)] * 2,
-            dma((8,)), dma((5,)), dma((5,)), dma((2, n // 2)), dma((2, n // 2 - 1)), dma((n, 2)), dma((3, n, 4)), dma((n, 4)),
-            dma((2,)), dma((2, cells)), dma((2, cells)), dma((2, 2)), dma((2, guests)), regular, regular,
+            dma((8,)), dma((5,)), dma((5,)), dma((3, n, 2)), dma((n, 2)), dma((3, n, 4)), dma((n, 4)),
+            dma((2,)), dma((2, cells)), dma((2, cells)), dma((2, 2)), dma((2, guests)), regular,
         ],
         compiler_params=pltpu.CompilerParams(
             collective_id=0, has_side_effects=True, vmem_limit_bytes=60 * 1024 * 1024
@@ -889,7 +881,7 @@
 
 def solution(mesh):
     n = mesh.shape["sp"]
-    body = grid_local if n == len(W_OWN[0]) and mesh.shape["tp"] == 4 else local
+    body = grid_local if n == len(CELLS[0]) and mesh.shape["tp"] == 4 else local
     return jax.shard_map(
         functools.partial(body, n),
         mesh=mesh,

time: 76.2 us -> 63.9 us (0.84)
  Pallas kernels: 72.2 us -> 59.7 us
    pallas_call x1, Pallas kernels: 72.2 us -> 59.7 us  [grid_local(): pl.pallas_call(functools.partial(grid_kernel, n), out_shape=(jax.ShapeDty...]
where the time goes in v2:
time: 63.9 us; the launch traced here: 63.4 us
  Pallas kernels  59.7 us (93%)
  local copies, waits for them, and re-layouts  3.12 us (5%)
  between operations  0.64 us (1%)
    pallas_call x1, Pallas kernels, grid_local(): pl.pallas_call(functools.partial(grid_kernel, n), out_shape=(jax.ShapeDty...  59.7 us
    unnamed x2, local copies, waits for them, and re-layouts  3.12 us

profile of v2, /device:TPU:28, one launch (start us, length us, event | category | flops | bytes accessed | tf_op | source)
XLA Modules:
  0.0 63.4 jit_solution(12582153374857207183)
XLA Ops:
  0.6 59.7 %shard_map.131 = (bf16[64,4096]{1,0:T(8,128)(2,1)}, f32[2,256]{1,0:T(2,128)}) custom-call(bf16[64,4096]{1,0:T(8,128)(2,1)} %tok_ref.1, f32[1,4096]{1,0:T(1,128)} %bitcast.3, bf16[4096,256]{1,0:T(8,128)(2,1)} %wq_hbm.1, bf16[4096,128]{1,0:T(8,128)(2,1)} %wk_hbm.1, bf16[4096,128]{1,0:T(8,128)(2,1)} %wv_hbm.1, f32[1,2]{1,0:T(1,128)} %bitcast.5, ...), custom_call_target="tpu_custom_call" | custom-call | tf_op jit(solution)/shard_map/pallas_call | solution.py:842
  60.3 1.9 %copy.16 = bf16[64,4096]{1,0:T(8,128)(2,1)} copy(bf16[64,4096]{1,0:T(8,128)(2,1)} %get-tuple-element.8) | data formatting | bytes 1048576
  62.2 1.3 %copy.17 = f32[256,2]{0,1:T(2,128)} copy(f32[256,2]{0,1:T(2,128)} %bitcast.4) | data formatting | bytes 4096

commit v3 on v2

--- a/solution.py
+++ b/solution.py
@@ -14,91 +14,114 @@
 BF16 = jnp.bfloat16
 MESH = pl.DeviceIdType.MESH
 NT = (((1,), (1,)), ((), ()))
-EVENTS = [[(10, 138, 270, 398, 526, 646, 780, 908), (-1, -1, -1, -1, -1, 664, -1, -1)],
- [(74, 194, 330, 450, 586, 706, 840, 924),
-  (26, 154, 278, 414, 542, 662, 796, -1),
-  (-1, -1, 296, -1, -1, 680, -1, -1)],
- [],
- [(-1, 168, 292, 428, 548, 692, 804, 940)],
- [(-1, -1, -1, -1, -1, 393, -1, -1)],
- [(42, 162, 290, 418, 554, 674, 808, -1), (-1, -1, 312, -1, -1, -1, -1, -1)],
- [(-1, 184, 75, 203, 331, 459, 585, 713), (-1, -1, 308, 436, 564, 517, 820, 948)],
- [(58, 178, 306, 440, 562, 409, 824, 952),
-  (-1, 393, 517, 434, 265, 690, 901, 773),
-  (-1, -1, 553, 645, 773, 901, -1, 649)],
- [(90, 210, 346, 466, 75, 203, 329, 457),
-  (131, 3, 405, 648, 602, 722, 856, 789),
-  (265, 425, -1, 661, 677, 917, 917, -1)],
- [],
- [(-1, 441, 533, 293, 789, 933, 537, 665), (-1, -1, -1, -1, -1, 425, 933, 805)],
- [(147, 19, 3, 131, -1, -1, -1, -1), (281, -1, -1, -1, -1, -1, -1, -1)],
- [(-1, -1, 569, 664, -1, -1, -1, -1)],
- [(-1, -1, 91, 219, 347, 475, 73, 201)],
- [(313, 649, 19, 147, 805, 773, -1, -1), (-1, -1, 548, 693, -1, -1, -1, -1)],
- [(-1, 65, 57, 321, 258, 577, 601, 729),
-  (-1, 81, 35, 337, 281, 593, 345, 833),
-  (-1, -1, 564, -1, 821, -1, 949, 849),
-  (-1, -1, 681, -1, 449, -1, 553, -1),
-  (-1, -1, 193, -1, 465, -1, 645, -1),
-  (-1, -1, 209, -1, -1, -1, 705, -1),
-  (-1, -1, -1, -1, -1, -1, 721, -1)],
- [(-1, -1, 676, 696, 91, 386, 569, -1), (-1, -1, -1, -1, 274, 441, -1, -1), (-1, -1, -1, -1, 297, -1, -1, -1)],
- [(-1, -1, -1, 517, 917, 789, 89, 473),
-  (-1, -1, -1, 163, 290, 321, 449, 821),
-  (-1, -1, -1, 905, 313, 337, 465, 681),
-  (-1, -1, -1, 65, 193, -1, -1, 577),
-  (-1, -1, -1, 81, 209, -1, -1, 593)],
- [(-1, -1, -1, -1, -1, 219, -1, 697), (-1, -1, -1, -1, -1, 514, -1, -1), (-1, -1, -1, -1, -1, 137, -1, -1)],
- [(-1, -1, -1, -1, -1, 805, 297, 217),
-  (-1, -1, -1, -1, -1, 402, 193, 321),
-  (-1, -1, -1, -1, -1, 65, 209, 337),
-  (-1, -1, -1, -1, -1, 81, -1, -1)],
- [],
- [(-1, -1, -1, -1, -1, -1, -1, 393),
-  (-1, -1, -1, -1, -1, -1, -1, 565),
-  (-1, -1, -1, -1, -1, -1, -1, 65),
-  (-1, -1, -1, -1, -1, -1, -1, 81)],
- [(-1, -1, 50, 179, 403, 277, -1, 425), (-1, -1, -1, 549, 9, -1, -1, -1), (-1, -1, -1, -1, 949, -1, -1, -1)],
- [(161, 401, -1, 937, -1, 418, -1, -1), (177, -1, -1, -1, -1, 169, -1, -1), (-1, -1, -1, -1, -1, 945, -1, -1)],
- [(289, 665, 147, 19, -1, -1, 313, -1), (-1, 33, -1, 673, -1, -1, 513, -1), (-1, 49, -1, -1, -1, -1, -1, -1)],
- [(385, 34, 825, 35, 306, 817, 657, 513),
-  (401, 697, 385, 1, 385, -1, 673, 529),
-  (417, 257, 417, 49, 417, -1, 689, 545),
-  (433, 273, 433, -1, 433, -1, -1, -1),
-  (-1, 289, -1, -1, -1, -1, -1, -1),
-  (-1, 305, -1, -1, -1, -1, -1, -1)],
- [(162, 531, 691, 769, 434, 259, 441, 257),
-  (537, 513, 769, 785, 57, 185, 257, 273),
-  (178, 545, 785, 801, 897, 145, 273, 289),
-  (569, 561, 801, 817, 929, -1, -1, 305),
-  (513, -1, -1, -1, -1, -1, -1, -1),
-  (545, -1, -1, -1, -1, -1, -1, -1)],
- [(681, 673, 641, -1, 17, 274, 385, 401),
-  (641, -1, 657, -1, 33, 289, 401, 433),
-  (657, -1, -1, -1, -1, 305, 417, -1),
-  (689, -1, -1, -1, -1, -1, -1, -1)],
- [(-1, -1, 953, 257, 641, 529, -1, -1),
-  (-1, -1, 897, 273, 657, 545, -1, -1),
-  (-1, -1, 913, 305, 689, 561, -1, -1),
-  (-1, -1, 929, -1, -1, -1, -1, -1)],
- [(-1, -1, -1, 529, 129, 1, -1, -1),
-  (-1, -1, -1, 561, 145, 17, -1, -1),
-  (-1, -1, -1, -1, 161, 33, -1, -1),
-  (-1, -1, -1, -1, 177, 49, -1, -1)],
- [(-1, -1, -1, 913, -1, -1, -1, -1), (-1, -1, -1, 945, -1, -1, -1, -1)],
- [(-1, -1, 129, -1, -1, -1, -1, -1), (-1, -1, 161, -1, -1, -1, -1, -1), (-1, -1, 177, -1, -1, -1, -1, -1)],
- []]
+EVENTS = [[(8, 18), (136, 146), (266, 276), (398,), (518, 536), (648, 662), (780,), (908,)],
+ [(74, 24, 34),
+  (194, 152, 162),
+  (330, 274, 292, 312),
+  (450, 410, 420),
+  (586, 530, 548, 568),
+  (706, 686),
+  (840, 792, 820),
+  (920, 932)],
+ [(), (), (), (), (), (), (), ()],
+ [(), (), (), (), (), (), (), ()],
+ [(), (184,), (308,), (436,), (), (692,), (), (956,)],
+ [(), (), (), (), (), (), (), ()],
+ [(40, 50),
+  (178,),
+  (290, 521, 75, 389),
+  (418, 203, 261),
+  (546, 265, 645, 331),
+  (690, 905, 459, 533),
+  (808, 585),
+  (713, 773)],
+ [(90, 56, 131), (210, 3, 425), (346,), (466,), (602, 821), (722, 937), (856, 917), (665,)],
+ [(297,),
+  (441,),
+  (405, 306, 553, 645),
+  (661, 434, 169, 697, 677),
+  (562, 281),
+  (900, 387, 409, 932),
+  (521,),
+  (789, 681)],
+ [(106, 419),
+  (226, 35, 265),
+  (91, 362),
+  (219, 482),
+  (75, 347, 618, 917),
+  (203, 475, 738),
+  (329, 601, 872),
+  (457, 729, 805)],
+ [(), (), (), (), (), (), (), ()],
+ [(), (), (825,), (185,), (), (), (661,), ()],
+ [(), (), (), (), (), (), (), ()],
+ [(313,), (), (165,), (517,), (933,), (565,), (), ()],
+ [(), (665,), (), (), (920,), (793,), (537,), (697,)],
+ [(), (), (), (), (), (), (), ()],
+ [(),
+  (291, 681, 65, 81, 97),
+  (107, 19, 137, 693, 35, 917, 51, 193, 209, 225),
+  (235, 147, 533, 321, 337, 353),
+  (91, 363, 107, 642, 661, 313, 291, 789, 25, 449, 465, 481),
+  (219, 949, 491, 235, 259, 577, 593, 609),
+  (73, 345, 617, 89, 361, 105, 693, 553, 705, 721, 737),
+  (517, 201, 473, 745, 833, 849, 865)],
+ [(), (), (), (178, 9), (930,), (), (), (217,)],
+ [(),
+  (),
+  (),
+  (901, 2, 569, 65, 81, 97),
+  (193, 209, 225),
+  (419, 773, 809, 277, 153, 321, 337, 353),
+  (569, 449, 465, 481),
+  (489, 233, 393, 577, 593, 609)],
+ [(), (), (), (), (), (274,), (), ()],
+ [(), (), (), (), (), (65, 81, 97), (193, 209, 225), (265, 321, 337, 353)],
+ [(), (), (), (), (), (), (649,), ()],
+ [(), (), (), (), (), (), (), (65, 81, 97)],
+ [(), (), (162, 933), (), (403, 41, 805), (435, 804, 185), (), (425,)],
+ [(385, 401, 433), (17, 49), (1,), (549,), (), (), (), (281, 529, 545, 561)],
+ [(408, 257, 273),
+  (521, 537, 385, 401),
+  (130, 793, 565, 417, 433),
+  (546, 953, 129),
+  (306, 57, 673, 689),
+  (913,),
+  (297, 389, 673),
+  (441, 641)],
+ [(649, 434, 145, 161, 177),
+  (905, 643, 553, 689),
+  (434, 949, 657, 673),
+  (933, 819, 777, 948, 130, 273, 289, 305),
+  (149, 769),
+  (916, 307, 9, 513, 545),
+  (897, 929, 945),
+  (289, 305)],
+ [(697, 675, 657),
+  (913, 929, 945),
+  (946, 769, 801),
+  (641,),
+  (169, 129, 177),
+  (21, 819),
+  (409, 421, 257, 273, 305),
+  (817,)],
+ [(921, 531, 569, 899, 929, 945), (561,), (), (276, 290, 785, 801), (1,), (53, 33), (433,), (401,)],
+ [(513, 545), (273, 305), (529,), (), (), (), (), ()],
+ [(), (), (145, 177), (913,), (), (129, 161), (), ()],
+ [(), (), (897,), (17, 33, 49), (897, 945), (), (), ()],
+ [(), (), (), (), (385, 417, 433), (289,), (), ()],
+ [(), (), (), (), (), (), (), ()]]
 CELLS = [(0, 1, 2, 3, 4, 5, 6, 7),
- (1, 3, 4, 1, 6, 7, 7, 5),
- (2, 0, 0, 5, 2, 3, 4, 6),
- (3, 2, 3, 0, 3, 6, 5, 4),
- (4, 4, 14, 14, 7, 1, 2, 2),
- (5, 5, 5, 6, 0, 2, 3, 3),
- (-1, -1, 23, 2, 5, 4, -1, -1),
- (-1, -1, 6, 4, 1, 0, -1, -1),
- (-1, -1, 7, 23, 8, 8, -1, -1),
- (-1, -1, 1, 7, 17, 17, -1, -1)]
-CELL_BACK = [(6, 6, -1, -1, -1, -1, 0, 0), (7, 7, -1, -1, -1, -1, 1, 1)]
+ (3, 0, 0, 4, 2, 3, 4, 4),
+ (2, 3, 3, 1, 5, 7, 5, 5),
+ (1, 5, 5, 2, 6, 4, 7, 2),
+ (5, 7, 14, 5, 1, 6, 2, 6),
+ (7, 4, 6, 14, 0, 8, 3, 3),
+ (4, 2, 4, 6, 8, 0, -1, -1),
+ (-1, -1, 1, 7, 17, 17, -1, -1),
+ (-1, -1, 7, 0, 7, 1, -1, -1),
+ (-1, -1, -1, -1, 3, 2, -1, -1)]
+CELL_BACK = [(6, 6, -1, -1, -1, -1, 0, 0), (-1, -1, -1, -1, -1, -1, 1, 1)]
 
 
 def softplus(z):
@@ -470,11 +493,17 @@
         out = out.transpose(1, 0, 2).reshape(rows, n * feats)
     return (out, logw.T)
 
+def soft_plus(z):
+    u = jnp.exp(-jnp.abs(z))
+    small = u - (u * u) * (0.5 - u * (1.0 / 3.0))
+    return jnp.maximum(z, 0.0) + jnp.where(u < 0.005, small, jnp.log(1.0 + u))
+
+
 def grid_kernel(
     n,
-    tok_ref, gain_ref, wq_hbm, wk_hbm, wv_hbm, shift_ref, wb_hbm, wc_hbm, wu_hbm, taps_ref, woa_ref, woc_ref,
+    tok_hbm, gain_hbm, wq_hbm, wk_hbm, wv_hbm, shift_hbm, wb_hbm, wc_hbm, wu_hbm, taps_hbm, woa_ref, woc_ref,
     out_ref, logw_ref,
-    wq, wkv, wb, wc, wu, xall, normed, q_sc, kv, wo, gate_sc, prod_sc, prev, ext, acts, acc, suffix,
+    gain_ref, shift_ref, taps_ref, wq, wkv, wb, wc, wu, xall, normed, q_sc, kv, wo, gate_sc, prod_sc, prev, ext, acts, acc, suffix,
     snd, keep, d2d, xsnd, xrcv, gsnd, grcv,
     load_sem, tok_ssem, tok_rsem, kv_ssem, kv_rsem, w_ssem, w_rsem, halo_sem, d2d_sem, x_sem,
     act_sem, ret_sem, near_by,
@@ -492,12 +521,12 @@
     levels = n // 2
     has_up, has_down = z < levels - 1, z > 0
     outer = jnp.logical_or(z == 0, z == levels - 1)
-    rows = tok_ref.shape[0]
+    rows = tok_hbm.shape[0]
     toks = 4 * rows
     half = rows // 2
     fpart = wo.shape[2] // 2
     feats = wo.shape[2]
-    heads = q_sc.shape[1] // HEAD_DIM
+    heads = q_sc.shape[0] // toks
     kv_cols = kv.shape[4]
     grouping = heads // (kv_cols // HEAD_DIM)
 
@@ -523,6 +552,14 @@
     own_loads = [
         pltpu.make_async_copy(src, wo.at[sp, i], load_sem.at[6 + i]) for i, src in enumerate((woa_ref, woc_ref))
     ]
+    tok_loads = [
+        pltpu.make_async_copy(tok_hbm.at[pl.ds(c * half, half)], xall.at[t, pl.ds(c * half, half)], load_sem.at[8 + c])
+        for c in range(2)
+    ]
+    small_loads = [
+        pltpu.make_async_copy(src, dst, load_sem.at[10 + i])
+        for i, (src, dst) in enumerate(((gain_hbm, gain_ref), (shift_hbm, shift_ref), (taps_hbm, taps_ref)))
+    ]
     barrier = pltpu.get_barrier_semaphore()
 
     def tell(sem, place):
@@ -537,7 +574,7 @@
         pl.semaphore_signal(barrier, inc=1, device_id={"tp": place}, device_id_type=MESH)
     tell(barrier, side)
     tell_column(barrier)
-    for load in (*own_loads, *loads):
+    for load in (*tok_loads, *own_loads, *small_loads, *loads):
         load.start()
     pl.semaphore_wait(barrier, 3 + column)
 
@@ -547,67 +584,88 @@
         )
 
     to_far = [
-        push(tok_ref.at[pl.ds(c * half, half)], xall.at[t, pl.ds(c * half, half)], tok_ssem.at[c], tok_rsem.at[c], {"tp": far})
+        push(xall.at[t, pl.ds(c * half, half)], xall.at[t, pl.ds(c * half, half)], tok_ssem.at[c], tok_rsem.at[c], {"tp": far})
         for c in range(2)
     ]
-    to_near = push(tok_ref, xall.at[t], tok_ssem.at[2], tok_rsem.at[2], {"tp": near})
+    to_near = push(xall.at[t], xall.at[t], tok_ssem.at[2], tok_rsem.at[2], {"tp": near})
     relay = [
         push(xall.at[far, pl.ds(c * half, half)], xall.at[far, pl.ds(c * half, half)], tok_ssem.at[3 + c], tok_rsem.at[3 + c], {"tp": near})
         for c in range(2)
     ]
-    for copy in to_far:
+    for load, copy in zip(tok_loads, to_far):
+        load.wait()
         copy.start()
     to_near.start()
     tell_column(near_by)
 
     early = t // 2
 
-    def w_copy(h, c, d):
-        view = wo.at[h, c // 2, pl.ds(pl.multiple_of((c % 2) * fpart, fpart), fpart)]
-        return push(view, view, w_ssem.at[d, h, c], w_rsem.at[h, c], {"sp": ways[d]})
-
-    def kv_copy(h, c, d):
-        view = kv.at[h, early + (c - 4) * (1 - 2 * early)]
-        return push(view, view, kv_ssem.at[d, h, c - 4], kv_rsem.at[h, c - 4], {"sp": ways[d]})
-
-    def event(vals, arrive, leave):
-        code = pick(vals)
-        h, c = code // 128, code // 16 % 8
-        for copy_of, low, high in ((w_copy, 0, 4), (kv_copy, 4, 6)):
-            mine = [v for v in vals if v >= 0 and low <= v // 16 % 8 < high]
-            if not mine:
-                continue
-            live = jnp.logical_and(code >= 16 * low, c < high) if low == 0 else c >= low
-            live = jnp.logical_and(live, code >= 0)
-
-            @pl.when(live)
-            def _():
-                if arrive and any(v % 2 for v in mine):
-                    pl.when(code % 2 == 1)(lambda: copy_of(h, c, 0).wait_recv())
-                for d in range(3):
-                    if any(v // 2 // 2**d % 2 for v in mine):
-                        pl.when(code // 2 // 2**d % 2 == 1)(lambda d=d: leave(copy_of(h, c, d)))
+    def hop_copy(site, h, c, d):
+        if c < 4:
+            view = wo.at[h, c // 2, pl.ds(c % 2 * fpart, fpart)]
+            sems = (w_ssem.at[d, h, c], w_rsem.at[h, c])
+        else:
+            view = kv.at[h, early] if c == 4 else kv.at[h, 1 - early, :, pl.ds((c - 5) * rows, rows)]
+            sems = (kv_ssem.at[d, h, c - 4], kv_rsem.at[h, c - 4])
+        return push(view, view, *sems, {"sp": (site + 2, site - 2, site ^ 1)[d]})
+
+    def at_site(bodies, low=0, high=n):
+        if all(body is None for body in bodies[low:high]):
+            return
+        if high - low == 1:
+            bodies[low]()
+            return
+        mid = (low + high) // 2
+        lax.cond(sp < mid, lambda: at_site(bodies, low, mid), lambda: at_site(bodies, mid, high))
+
+    def events(point, arrive, leave):
+        def body_of(site, codes):
+            def body():
+                for code in codes:
+                    h, c = code // 128, code // 16 % 8
+                    if arrive and code % 2:
+                        hop_copy(site, h, c, 2).wait_recv()
+                    for d in range(3):
+                        if code // 2 // 2**d % 2:
+                            leave(hop_copy(site, h, c, d))
+
+            return body if codes else None
+
+        at_site([body_of(site, codes) for site, codes in enumerate(EVENTS[point])])
 
     def pump(point):
-        for vals in EVENTS[point]:
-            event(vals, True, lambda copy: copy.start())
+        events(point, True, lambda copy: copy.start())
 
     for load in own_loads:
         load.wait()
     pump(0)
+    for load in small_loads:
+        load.wait()
 
     def dot(w):
         return jnp.dot(normed[...], w[...], preferred_element_type=F32)
 
-    def project_kv(groups, pair):
-        for i, g in enumerate(groups):
-            x = (tok_ref[...] if g is None else xall[g]).astype(F32)
-            inverse = lax.rsqrt(jnp.mean(x * x, axis=-1, keepdims=True) + 1e-06)
-            at = rows * (t % 2 if i == 0 else 1 - t % 2)
-            normed[pl.ds(pl.multiple_of(at, rows), rows)] = (x * inverse * gain_ref[...]).astype(BF16)
+    def normalize(g, same, low, count):
+        x = xall[g, pl.ds(low, count)].astype(F32)
+        inverse = lax.rsqrt(jnp.mean(x * x, axis=-1, keepdims=True) + 1e-06)
+        at = rows * (t % 2 if same else 1 - t % 2) + low
+        normed[pl.ds(pl.multiple_of(at, half), count)] = (x * inverse * gain_ref[...]).astype(BF16)
+
+    def project_early():
+        normalize(t, True, 0, rows)
+        normalize(near, False, 0, rows)
         both = dot(wkv).astype(BF16)
-        kv[sp, pair, 0] = both[:, :kv_cols]
-        kv[sp, pair, 1] = both[:, kv_cols:]
+        kv[sp, early, 0] = both[:, :kv_cols]
+        kv[sp, early, 1] = both[:, kv_cols:]
+
+    def project_late(c):
+        normalize(far, True, c * half, half)
+        normalize(diag, False, c * half, half)
+        some = jnp.concatenate([normed[pl.ds(c * half, half)], normed[pl.ds(rows + c * half, half)]], axis=0)
+        both = jnp.dot(some, wkv[...], preferred_element_type=F32).astype(BF16)
+        at = pl.ds(c * rows, rows)
+        kv[sp, 1 - early, 0, at] = both[:, :kv_cols]
+        kv[sp, 1 - early, 1, at] = both[:, kv_cols:]
 
     def project_rest(pair, points):
         at = pl.ds(pl.multiple_of(pair * 2 * rows, 2 * rows), 2 * rows)
@@ -615,7 +673,10 @@
         pump(points[0])
         prod_sc[at] = (gate * dot(wu).astype(BF16).astype(F32)).astype(BF16)
         pump(points[1])
-        q_sc[at] = dot(wq).astype(BF16)
+        queries = dot(wq).astype(BF16)
+        for h in range(heads):
+            to = pl.ds(pl.multiple_of(h * toks + pair * 2 * rows, 2 * rows), 2 * rows)
+            q_sc[to] = queries[:, h * HEAD_DIM : (h + 1) * HEAD_DIM]
         pump(points[2])
         gate_sc[at] = dot(wb).astype(BF16)
         pump(points[3])
@@ -623,56 +684,65 @@
     to_near.wait_recv()
     for load in loads[:2]:
         load.wait()
-    project_kv((None, near), early)
+    project_early()
     pump(1)
     for load in loads[2:]:
         load.wait()
     project_rest(early, (2, 3, 4, 5))
-    pump(6)
-    to_far[0].wait_recv()
-    relay[0].start()
-    pump(7)
-    to_far[1].wait_recv()
-    relay[1].start()
     for c in range(2):
+        pump(6 + 2 * c)
+        to_far[c].wait_recv()
+        relay[c].start()
         relay[c].wait_recv()
-    project_kv((far, diag), 1 - early)
-    pump(8)
-    project_rest(1 - early, (9, 10, 11, 12))
+        project_late(c)
+        pump(7 + 2 * c)
+    project_rest(1 - early, (10, 11, 12, 13))
     pl.semaphore_wait(near_by, column)
     halo = push(prod_sc.at[pl.ds(toks - HALO, HALO)], prev, halo_sem.at[0], halo_sem.at[1], {"sp": sp + 1})
     guard(sp < n - 1)(halo.start)
 
-    key_i = lax.broadcasted_iota(jnp.int32, (toks, toks), 0)
-    key_j = lax.broadcasted_iota(jnp.int32, (toks, toks), 1)
-    later = (key_i > key_j).astype(F32).astype(BF16)
+    def spot(index):
+        index = index % toks
+        pair, sub = index // (2 * rows), index % (2 * rows)
+        moved = sub % rows // half * rows + sub // rows * half + sub % half
+        return jnp.where(pair == early, index, pair * 2 * rows + moved)
+
+    later = spot(lax.broadcasted_iota(jnp.int32, (2 * toks, 1), 0)) > spot(lax.broadcasted_iota(jnp.int32, (1, toks), 1))
+    later = later.astype(F32).astype(BF16)
+    stacked = grouping * toks
+    query = lax.broadcasted_iota(jnp.int32, (stacked, 1), 0) % toks
+    causal = spot(lax.broadcasted_iota(jnp.int32, (1, toks), 1)) < query
+    head_of = lax.broadcasted_iota(jnp.int32, (stacked, 1), 0) // toks
     scale = HEAD_DIM ** (-0.5)
     order = (t, far, near, diag)
 
     def visit(slot, masked):
-        for h in range(heads):
-            cols = pl.ds(h * HEAD_DIM, HEAD_DIM)
-            kv_at = pl.ds((h // grouping) * HEAD_DIM, HEAD_DIM)
+        for g in range(heads // grouping):
+            at = pl.ds(g * stacked, stacked)
+            kv_at = pl.ds(g * HEAD_DIM, HEAD_DIM)
             keys = kv[slot, :, 0, :, kv_at].reshape(toks, HEAD_DIM)
             vals = kv[slot, :, 1, :, kv_at].reshape(toks, HEAD_DIM)
-            s = lax.dot_general(q_sc[:, cols], keys, NT, preferred_element_type=F32) * scale + shift_ref[0, h]
-            soft = softplus(s)
+            shift = shift_ref[0:1, g * grouping : g * grouping + 1]
+            for h in range(1, grouping):
+                shift = jnp.where(head_of < h, shift, shift_ref[0:1, g * grouping + h : g * grouping + h + 1])
+            s = lax.dot_general(q_sc[at], keys, NT, preferred_element_type=F32) * scale + shift
+            soft = soft_plus(s)
             if masked:
-                soft = jnp.where(key_j < key_i, soft, 0.0)
+                soft = jnp.where(causal, soft, 0.0)
             high = soft.astype(BF16)
             low = (soft - high.astype(F32)).astype(BF16)
-            after = jnp.dot(high, later, preferred_element_type=F32) + jnp.dot(low, later, preferred_element_type=F32)
+            after = jnp.dot(jnp.concatenate([high, low], axis=1), later, preferred_element_type=F32)
             weight = jnp.exp(s - soft - after)
             if masked:
-                weight = jnp.where(key_j < key_i, weight, 0.0)
+                weight = jnp.where(causal, weight, 0.0)
             part = jnp.dot(weight.astype(BF16), vals, preferred_element_type=F32)
-            total = jnp.broadcast_to(after[:, 0:1] + soft[:, 0:1], (toks, HEAD_DIM))
+            total = jnp.broadcast_to(after[:, 0:1] + soft[:, 0:1], (stacked, HEAD_DIM))
             if masked:
-                acc[:, cols] = part
-                suffix[h] = total
+                acc[at] = part
+                suffix[at] = total
             else:
-                acc[:, cols] += jnp.exp(-suffix[h]) * part
-                suffix[h] += total
+                acc[at] += jnp.exp(-suffix[at]) * part
+                suffix[at] += total
 
     def convolve():
         @pl.when(sp == 0)
@@ -693,23 +763,25 @@
         return push(acts.at[0, i], acts.at[1, i], act_sem.at[0, i], act_sem.at[1, i], {"sp": host})
 
     visit(sp, True)
-    pump(13)
+    pump(14)
     convolve()
     guard(outer)(lambda: act_copy(1).start())
-    pump(14)
+    pump(15)
     for i in range(1, n):
-        pump(14 + i)
+        pump(15 + i)
 
         @pl.when(sp >= i)
         def _():
             visit(sp - i, False)
 
     for h in range(heads):
-        spread = suffix[h].T[0:1, :]
+        for i, g in enumerate(order):
+            have = acc[pl.ds(pl.multiple_of(h * toks + g * rows, rows), rows)]
+            acts[0, 0, pl.ds(i * rows, rows), pl.ds(h * HEAD_DIM, HEAD_DIM)] = have.astype(BF16)
+    guard(outer)(lambda: act_copy(0).start())
+    for h in range(heads):
+        spread = suffix[pl.ds(h * toks, toks)].T[0:1, :]
         logw_ref[h : h + 1, :] = jnp.log(jnp.maximum(1.0 - jnp.exp(-spread), 0.05))
-    for i, g in enumerate(order):
-        acts[0, 0, pl.ds(i * rows, rows)] = acc[pl.ds(pl.multiple_of(g * rows, rows), rows)].astype(BF16)
-    guard(outer)(lambda: act_copy(0).start())
 
     def d2d_copy(i):
         return push(snd.at[i], d2d.at[i], d2d_sem.at[0, i], d2d_sem.at[1, i], {"tp": near})
@@ -786,7 +858,7 @@
 
     steps = len(CELLS)
     for i in range(steps):
-        pump(22 + i)
+        pump(23 + i)
         first(i)
         if i >= 1:
             second(i - 1)
@@ -795,7 +867,7 @@
     second(steps - 1)
     for i in range(steps - 3, steps):
         third(i)
-    pump(22 + steps)
+    pump(23 + steps)
     for r in range(len(CELL_BACK)):
         @pl.when(pick(CELL_BACK[r]) >= 0)
         def _():
@@ -805,9 +877,8 @@
     for copy in (*to_far, to_near, *relay):
         copy.wait_send()
     guard(sp < n - 1)(halo.wait_send)
-    for slots in EVENTS:
-        for vals in slots:
-            event(vals, False, lambda copy: copy.wait_send())
+    for point in range(len(EVENTS)):
+        events(point, False, lambda copy: copy.wait_send())
 
     @pl.when(outer)
     def _():
@@ -820,6 +891,22 @@
             d2d_copy(i).wait_send()
             x_copy(i).wait_send()
             kinds(i, lambda j: None, lambda j, r: ret_copy(r).wait_send())
+
+
+def finish_kernel(out_ref, logw_ref, out, logw):
+    out[...] = out_ref[...]
+    logw[...] = logw_ref[...]
+
+
+def finish(out, logw):
+    vmem = pl.BlockSpec(memory_space=pltpu.VMEM)
+    out, logw = pl.pallas_call(
+        finish_kernel,
+        out_shape=(jax.ShapeDtypeStruct(out.shape, out.dtype), jax.ShapeDtypeStruct(logw.shape, logw.dtype)),
+        in_specs=[vmem, vmem],
+        out_specs=(vmem, vmem),
+    )(out, logw)
+    return (out, logw.T)
 
 
 def grid_local(
@@ -835,7 +922,6 @@
     cells = len(CELLS)
     guests = len(CELL_BACK)
     vmem = pl.BlockSpec(memory_space=pltpu.VMEM)
-    smem = pl.BlockSpec(memory_space=pltpu.SMEM)
     hbm = pl.BlockSpec(memory_space=pl.ANY)
     dma = pltpu.SemaphoreType.DMA
     regular = pltpu.SemaphoreType.REGULAR
@@ -845,15 +931,18 @@
             jax.ShapeDtypeStruct((rows, n * feats), BF16),
             jax.ShapeDtypeStruct((heads, toks), F32),
         ),
-        in_specs=[vmem, vmem, hbm, hbm, hbm, smem, hbm, hbm, hbm, vmem, hbm, hbm],
+        in_specs=[hbm] * 12,
         out_specs=(vmem, vmem),
         scratch_shapes=[
+            pltpu.VMEM((1, d), F32),
+            pltpu.VMEM((1, heads), F32),
+            pltpu.VMEM(conv_kernel.shape, F32),
             pltpu.VMEM(w_query.shape, BF16),
             pltpu.VMEM((d, 2 * kv_cols), BF16),
             *[pltpu.VMEM(w.shape, BF16) for w in (w_conv_b, w_conv_c, w_conv_u)],
             pltpu.VMEM((4, rows, d), BF16),
             pltpu.VMEM((2 * rows, d), BF16),
-            pltpu.VMEM((toks, w_query.shape[1]), BF16),
+            pltpu.VMEM((heads * toks, HEAD_DIM), BF16),
             pltpu.VMEM((n, 2, 2, 2 * rows, kv_cols), BF16),
             pltpu.VMEM((n, 2, feats, att_cols), BF16),
             pltpu.VMEM((toks, conv_cols), BF16),
@@ -861,12 +950,11 @@
             pltpu.VMEM((HALO, conv_cols), BF16),
             pltpu.VMEM((toks + HALO, conv_cols), F32),
             pltpu.VMEM((2, 2, toks, att_cols), BF16),
-            pltpu.VMEM((toks, att_cols), F32),
-            pltpu.VMEM((heads, toks, HEAD_DIM), F32),
+            *[pltpu.VMEM((heads * toks, HEAD_DIM), F32)] * 2,
             *[pltpu.VMEM((cells, 2 * rows, feats), BF16)] * 3,
             *[pltpu.VMEM((cells, rows, feats), BF16)] * 2,
             *[pltpu.VMEM((guests, rows, feats), BF16)] * 2,
-            dma((8,)), dma((5,)), dma((5,)), dma((3, n, 2)), dma((n, 2)), dma((3, n, 4)), dma((n, 4)),
+            dma((13,)), dma((5,)), dma((5,)), dma((3, n, 3)), dma((n, 3)), dma((3, n, 4)), dma((n, 4)),
             dma((2,)), dma((2, cells)), dma((2, cells)), dma((2, 2)), dma((2, guests)), regular,
         ],
         compiler_params=pltpu.CompilerParams(
@@ -876,7 +964,7 @@
         tokens, norm_gain.reshape(1, d), w_query, w_key, w_value, score_shift.reshape(1, heads),
         w_conv_b, w_conv_c, w_conv_u, conv_kernel, w_out_att, w_out_conv,
     )
-    return (out, logw.T)
+    return finish(out, logw)
 
 
 def solution(mesh):

time: 63.9 us -> 57.9 us (0.906)
  local copies, waits for them, and re-layouts: 3.12 us -> 0 us
  Pallas kernels: 59.7 us -> 56.8 us
    pallas_call x1, Pallas kernels: 59.7 us -> 54.9 us  [grid_local(): pl.pallas_call(functools.partial(grid_kernel, n), out_shape=(jax.ShapeDty...]
    unnamed x2 -> x0, local copies, waits for them, and re-layouts: 3.12 us -> none
    pallas_call x0 -> x1, Pallas kernels: none -> 1.87 us  [finish(): pl.pallas_call(finish_kernel, out_shape=(jax.ShapeDtypeStruct(out.shape,...]
where the time goes in v3:
time: 57.9 us; the launch traced here: 57.5 us
  Pallas kernels  56.8 us (98%)
  between operations  0.64 us (1%)
    pallas_call x1, Pallas kernels, grid_local(): pl.pallas_call(functools.partial(grid_kernel, n), out_shape=(jax.ShapeDty...  54.9 us
    pallas_call x1, Pallas kernels, finish(): pl.pallas_call(finish_kernel, out_shape=(jax.ShapeDtypeStruct(out.shape,...  1.87 us

profile of v3, /device:TPU:28, one launch (start us, length us, event | category | flops | bytes accessed | tf_op | source)
XLA Modules:
  0.0 57.5 jit_solution(17719013602298901617)
XLA Ops:
  0.6 54.9 %shard_map.131 = (bf16[64,4096]{1,0:T(8,128)(2,1)}, f32[2,256]{1,0:T(2,128)}) custom-call(bf16[64,4096]{1,0:T(8,128)(2,1)} %tok_hbm.1, f32[1,4096]{1,0:T(1,128)} %bitcast.3, bf16[4096,256]{1,0:T(8,128)(2,1)} %wq_hbm.1, bf16[4096,128]{1,0:T(8,128)(2,1)} %wk_hbm.1, bf16[4096,128]{1,0:T(8,128)(2,1)} %wv_hbm.1, f32[1,2]{1,0:T(1,128)} %bitcast.4, ...), custom_call_target="tpu_custom_call" | custom-call | tf_op jit(solution)/shard_map/pallas_call | solution.py:928
  55.6 1.9 %shard_map.132 = (bf16[64,4096]{1,0:T(8,128)(2,1)}, f32[2,256]{1,0:T(2,128)}) custom-call(bf16[64,4096]{1,0:T(8,128)(2,1)} %get-tuple-element.6.out_ref, f32[2,256]{1,0:T(2,128)} %get-tuple-element.7.logw_ref), custom_call_target="tpu_custom_call" | custom-call | tf_op jit(solution)/shard_map/pallas_call | solution.py:903

commit v4 on v3

--- a/solution.py
+++ b/solution.py
@@ -618,7 +618,7 @@
         mid = (low + high) // 2
         lax.cond(sp < mid, lambda: at_site(bodies, low, mid), lambda: at_site(bodies, mid, high))
 
-    def events(point, arrive, leave):
+    def events(lists, arrive, leave):
         def body_of(site, codes):
             def body():
                 for code in codes:
@@ -631,10 +631,16 @@
 
             return body if codes else None
 
-        at_site([body_of(site, codes) for site, codes in enumerate(EVENTS[point])])
+        at_site([body_of(site, codes) for site, codes in enumerate(lists)])
 
     def pump(point):
-        events(point, True, lambda copy: copy.start())
+        events(EVENTS[point], True, lambda copy: copy.start())
+
+    def drain(first_point, last_point):
+        merged = [
+            tuple(code for point in EVENTS[first_point:last_point] for code in point[site]) for site in range(n)
+        ]
+        events(merged, False, lambda copy: copy.wait_send())
 
     for load in own_loads:
         load.wait()
@@ -779,9 +785,6 @@
             have = acc[pl.ds(pl.multiple_of(h * toks + g * rows, rows), rows)]
             acts[0, 0, pl.ds(i * rows, rows), pl.ds(h * HEAD_DIM, HEAD_DIM)] = have.astype(BF16)
     guard(outer)(lambda: act_copy(0).start())
-    for h in range(heads):
-        spread = suffix[pl.ds(h * toks, toks)].T[0:1, :]
-        logw_ref[h : h + 1, :] = jnp.log(jnp.maximum(1.0 - jnp.exp(-spread), 0.05))
 
     def d2d_copy(i):
         return push(snd.at[i], d2d.at[i], d2d_sem.at[0, i], d2d_sem.at[1, i], {"tp": near})
@@ -865,6 +868,9 @@
         if i >= 3:
             third(i - 3)
     second(steps - 1)
+    for h in range(heads):
+        spread = suffix[pl.ds(h * toks, toks)].T[0:1, :]
+        logw_ref[h : h + 1, :] = jnp.log(jnp.maximum(1.0 - jnp.exp(-spread), 0.05))
     for i in range(steps - 3, steps):
         third(i)
     pump(23 + steps)
@@ -877,8 +883,7 @@
     for copy in (*to_far, to_near, *relay):
         copy.wait_send()
     guard(sp < n - 1)(halo.wait_send)
-    for point in range(len(EVENTS)):
-        events(point, False, lambda copy: copy.wait_send())
+    drain(0, len(EVENTS))
 
     @pl.when(outer)
     def _():

time: 57.9 us -> 57.9 us (level)
  no operation moved by 1% of the time
where the time goes in v4:
time: 57.9 us; the launch traced here: 57.5 us
  Pallas kernels  56.8 us (98%)
  between operations  0.64 us (1%)
    pallas_call x1, Pallas kernels, grid_local(): pl.pallas_call(functools.partial(grid_kernel, n), out_shape=(jax.ShapeDty...  54.9 us
    pallas_call x1, Pallas kernels, finish(): pl.pallas_call(finish_kernel, out_shape=(jax.ShapeDtypeStruct(out.shape,...  1.87 us

profile of v4, /device:TPU:28, one launch (start us, length us, event | category | flops | bytes accessed | tf_op | source)
XLA Modules:
  0.0 57.5 jit_solution(17662531025556845347)
XLA Ops:
  0.6 54.9 %shard_map.131 = (bf16[64,4096]{1,0:T(8,128)(2,1)}, f32[2,256]{1,0:T(2,128)}) custom-call(bf16[64,4096]{1,0:T(8,128)(2,1)} %tok_hbm.1, f32[1,4096]{1,0:T(1,128)} %bitcast.3, bf16[4096,256]{1,0:T(8,128)(2,1)} %wq_hbm.1, bf16[4096,128]{1,0:T(8,128)(2,1)} %wk_hbm.1, bf16[4096,128]{1,0:T(8,128)(2,1)} %wv_hbm.1, f32[1,2]{1,0:T(1,128)} %bitcast.4, ...), custom_call_target="tpu_custom_call" | custom-call | tf_op jit(solution)/shard_map/pallas_call | solution.py:933
  55.6 1.9 %shard_map.132 = (bf16[64,4096]{1,0:T(8,128)(2,1)}, f32[2,256]{1,0:T(2,128)}) custom-call(bf16[64,4096]{1,0:T(8,128)(2,1)} %get-tuple-element.6.out_ref, f32[2,256]{1,0:T(2,128)} %get-tuple-element.7.logw_ref), custom_call_target="tpu_custom_call" | custom-call | tf_op jit(solution)/shard_map/pallas_call | solution.py:908
